TPU v7x, 32 devices: a whole 2x2x4 slice. The times are simulated.
32 devices in a mesh: sp: 4 (over y, x), tp: 8 (over z, core).
Axes of the slice: x: 2, y: 2, z: 4, core: 2. Of those that a mesh axis runs over, the one named last changes fastest.
Arguments:
- queries: bfloat16 [4096, 1024], P('sp', 'tp'), may hold values from -18 to 18
- keys: bfloat16 [4096, 256], P('sp'), may hold values from -18 to 18
- values: bfloat16 [4096, 256], P('sp'), may hold values from -6 to 6
- sink_logits: float32 [16], P('tp'), may hold values from 3 to 7
- w_out: bfloat16 [1024, 2048], P('tp'), may hold values from -1.5 to 1.5
- residual: bfloat16 [4096, 2048], P(('sp', 'tp')), may hold values from -6 to 6
- norm_gain: float32 [2048], replicated, may hold values from 0.1 to 1.9
- expert_ids: int32 [4096, 4], P('sp'), may hold values from 0 to 15, all different within a row; in each aligned block of 1024 rows (0 to 1023, 1024 to 2047, ...) at most 512 rows name the same one
- expert_weights: float32 [4096, 4], P('sp'), may hold values from 0.1 to 1.5
- w_gate: bfloat16 [32, 768, 2048], P(('sp', 'tp')), may hold values from -0.125 to 0.125
- w_up: bfloat16 [32, 768, 2048], P(('sp', 'tp')), may hold values from -0.125 to 0.125
- w_down: bfloat16 [32, 768, 2048], P(('sp', 'tp')), may hold values from -0.15625 to 0.15625
- shared_gate: bfloat16 [512, 2048], P('tp'), may hold values from -0.125 to 0.125
- shared_up: bfloat16 [512, 2048], P('tp'), may hold values from -0.125 to 0.125
- shared_down: bfloat16 [512, 2048], P('tp'), may hold values from -0.25 to 0.25
Outputs:
- layer_out: bfloat16 [4096, 2048], P(('sp', 'tp'))
Inputs may be any that keep to these rules, and one draw needn't show every extreme that they name: `expert_ids`: each row names 4 different experts; in each aligned block of 1024 rows no expert is named by more than 512 rows.
All inputs are finite; a program needn't handle non-finite values.
Results may differ from a plain program's by a relative error of at most 0.02.
Values may be sent and summed in bfloat16 or wider, within the bound.
A program may use at most 128 MiB of HBM per device.

v0:
```python
import jax
import jax.numpy as jnp
from jax import lax
from jax.sharding import PartitionSpec as P

HD = 64
GROUP = 4
WINDOW = 128
TOPK = 4
CHUNKS = 2


def shifted(block, axis, distance):
    devices = range(lax.axis_size(axis))
    route = [(i - distance, i) for i in devices if i - distance in devices]
    return lax.ppermute(block, axis, route)


def from_partner(x, axis, apart):
    return lax.ppermute(x, axis, [(i, i ^ 1 << apart) for i in range(lax.axis_size(axis))])


def normalize(after_mix, norm_gain):
    values_f = after_mix.astype(jnp.float32)
    scale = lax.rsqrt(jnp.mean(values_f * values_f, axis=-1, keepdims=True) + 1e-06)
    return (values_f * scale * norm_gain).astype(jnp.bfloat16)


def lane_slots(route_ids, route_weights, targets, first_rank, half_cap):
    named = route_ids[:, :, None] == targets[None, None, :]
    named_f = jnp.sum(named.astype(jnp.float32), axis=1)
    weight = jnp.sum(jnp.where(named, route_weights[:, :, None], 0.0), axis=1)
    named_t = jnp.sum((route_ids.T[None] == targets[:, None, None]).astype(jnp.float32), axis=1)
    rows = route_ids.shape[0]
    steps = jnp.arange(rows)
    earlier = (steps[None, :] < steps[:, None]).astype(jnp.bfloat16)
    rank = jnp.dot(earlier, named_f.astype(jnp.bfloat16), preferred_element_type=jnp.float32)
    rank_t = jnp.einsum(
        "sq,pq->sp", named_t.astype(jnp.bfloat16), earlier, preferred_element_type=jnp.float32
    )
    place = jnp.where(named_f > 0, rank - first_rank, -1.0)
    place_t = jnp.where(named_t > 0, rank_t - first_rank, -1.0)
    slots = jnp.arange(half_cap, dtype=jnp.float32)
    picks, mixes = [], []
    for s in range(targets.shape[0]):
        hit_t = place_t[s : s + 1, :] == slots[:, None]
        picks.append(jnp.where(hit_t, 1.0, 0.0).astype(jnp.bfloat16))
        hit = place[:, s : s + 1] == slots[None, :]
        mixes.append(jnp.where(hit, weight[:, s : s + 1], 0.0).astype(jnp.bfloat16))
    return jnp.concatenate(picks, axis=0), jnp.concatenate(mixes, axis=1)


def body(
    queries,
    keys,
    values,
    sink_logits,
    w_out,
    residual,
    norm_gain,
    expert_ids,
    expert_weights,
    w_gate,
    w_up,
    w_down,
    shared_gate,
    shared_up,
    shared_down,
):
    other_gate, other_up, other_down = (from_partner(w[0], "tp", 0) for w in (w_gate, w_up, w_down))
    tp_count = lax.axis_size("tp")
    sp_count = lax.axis_size("sp")
    seq_rows = queries.shape[0]
    expert_count = sp_count * tp_count // 2
    capacity = max(2, 2 * seq_rows * TOPK // expert_count)
    local_heads = queries.shape[1] // HD
    kv_start = lax.axis_index("tp") * local_heads // GROUP * HD
    key_cols = lax.dynamic_slice_in_dim(keys, kv_start, HD, 1)
    value_cols = lax.dynamic_slice_in_dim(values, kv_start, HD, 1)
    rim = jnp.concatenate([keys[seq_rows - WINDOW :], values[seq_rows - WINDOW :]], axis=1)
    rim = shifted(rim, "sp", 1)
    rim_keys = lax.dynamic_slice_in_dim(rim, kv_start, HD, 1)
    rim_values = lax.dynamic_slice_in_dim(rim, kv_start + keys.shape[1], HD, 1)
    num_blocks = seq_rows // WINDOW
    key_blocks = key_cols.reshape(num_blocks, WINDOW, HD)
    value_blocks = value_cols.reshape(num_blocks, WINDOW, HD)
    keys_ext = jnp.concatenate(
        [jnp.concatenate([rim_keys[None], key_blocks[:-1]], axis=0), key_blocks], axis=1
    )
    values_ext = jnp.concatenate(
        [jnp.concatenate([rim_values[None], value_blocks[:-1]], axis=0), value_blocks], axis=1
    )
    query_blocks = queries.reshape(num_blocks, WINDOW, local_heads, HD)
    scores = jnp.einsum(
        "nqhd,nsd->nhqs", query_blocks, keys_ext, preferred_element_type=jnp.float32
    ) * HD ** (-0.5)
    query_pos = jnp.arange(WINDOW)[:, None] + WINDOW
    key_pos = jnp.arange(2 * WINDOW)[None, :]
    in_band = (key_pos <= query_pos) & (key_pos > query_pos - WINDOW)
    absolute = (
        lax.axis_index("sp") * seq_rows
        + jnp.arange(num_blocks)[:, None, None] * WINDOW
        + key_pos[None]
        - WINDOW
    )
    allowed = in_band[None] & (absolute >= 0)
    scores = jnp.where(allowed[:, None], scores, -jnp.inf)
    sink_col = jnp.broadcast_to(sink_logits[None, :, None, None], scores.shape[:-1] + (1,))
    combined = jnp.concatenate([scores, sink_col], axis=-1)
    row_max = jnp.max(combined, axis=-1, keepdims=True)
    exps = jnp.exp(combined - row_max)
    weights = (exps[..., :-1] / jnp.sum(exps, axis=-1, keepdims=True)).astype(jnp.bfloat16)
    attended = jnp.einsum("nhqs,nsd->nqhd", weights, values_ext, preferred_element_type=jnp.float32)
    attended = attended.astype(jnp.bfloat16).reshape(seq_rows, local_heads * HD)
    head_rows = lax.all_to_all(attended, "tp", split_axis=0, concat_axis=1, tiled=True)
    head_rows, other_gate, other_up, other_down = lax.optimization_barrier(
        (head_rows, other_gate, other_up, other_down)
    )
    projected = jnp.dot(
        head_rows,
        lax.all_gather(w_out, "tp", axis=0, tiled=True),
        preferred_element_type=jnp.float32,
    )
    after_mix = (residual.astype(jnp.float32) + projected).astype(jnp.bfloat16)
    normed = normalize(after_mix, norm_gain)
    tp_index = lax.axis_index("tp")
    lanes = tp_count // 2
    lane = tp_index // 2
    keep = tp_index % 2
    half_cap = capacity // 2
    targets = jnp.arange(sp_count, dtype=jnp.int32) * lanes + lane
    first_rank = (keep * half_cap).astype(jnp.float32)
    pick, mix = lane_slots(expert_ids, expert_weights, targets, first_rank, half_cap)
    width = after_mix.shape[1]
    step = width // CHUNKS
    gates = [(w_gate[0], w_up[0]), (other_gate, other_up)]
    downs = [w_down[0], other_down]
    sums = [[0.0, 0.0] for _ in gates]
    shared = [0.0, 0.0]
    for c in range(CHUNKS):
        cols = slice(c * step, (c + 1) * step)
        rows = lax.all_gather(normed[:, cols], "tp", axis=0, tiled=True)
        outgoing = jnp.dot(pick, rows, preferred_element_type=jnp.float32).astype(jnp.bfloat16)
        arrived = lax.all_to_all(
            outgoing.reshape(sp_count, half_cap, step), "sp", split_axis=0, concat_axis=0, tiled=True
        ).reshape(sp_count * half_cap, step)
        for total, pair in zip(sums, gates):
            for n, w in enumerate(pair):
                total[n] = total[n] + jnp.einsum(
                    "td,fd->tf", arrived, w[:, cols], preferred_element_type=jnp.float32
                )
        for n, w in enumerate((shared_gate, shared_up)):
            shared[n] = shared[n] + jnp.einsum(
                "td,fd->tf", rows, w[:, cols], preferred_element_type=jnp.float32
            )
    shared_hidden = (jax.nn.silu(shared[0]) * shared[1]).astype(jnp.bfloat16)
    hidden = [(jax.nn.silu(g) * u).astype(jnp.bfloat16) for g, u in sums]
    pieces = []
    outs = []
    for c in range(CHUNKS):
        cols = slice(c * step, (c + 1) * step)
        expert_out = sum(
            jnp.dot(h, w[:, cols], preferred_element_type=jnp.float32) for h, w in zip(hidden, downs)
        ).astype(jnp.bfloat16)
        outs.append(expert_out.reshape(sp_count, half_cap, step))
    for c in range(CHUNKS):
        cols = slice(c * step, (c + 1) * step)
        held = lax.all_to_all(outs[c], "sp", split_axis=0, concat_axis=0, tiled=True)
        if c + 1 < CHUNKS:
            held, outs[c + 1] = lax.optimization_barrier((held, outs[c + 1]))
        held = held.reshape(sp_count * half_cap, step)
        part = jnp.dot(shared_hidden, shared_down[:, cols], preferred_element_type=jnp.float32)
        part = part + jnp.dot(mix, held, preferred_element_type=jnp.float32)
        pieces.append(
            lax.psum_scatter(part.astype(jnp.bfloat16), "tp", scatter_dimension=0, tiled=True)
        )
    moe_sum = jnp.concatenate(pieces, axis=1)
    return (after_mix.astype(jnp.float32) + moe_sum.astype(jnp.float32)).astype(jnp.bfloat16)


def solution(mesh):
    return jax.shard_map(
        body,
        mesh=mesh,
        in_specs=(
            P("sp", "tp"),
            P("sp", None),
            P("sp", None),
            P("tp"),
            P("tp", None),
            P(("sp", "tp"), None),
            P(),
            P("sp", None),
            P("sp", None),
            P(("sp", "tp"), None, None),
            P(("sp", "tp"), None, None),
            P(("sp", "tp"), None, None),
            P("tp", None),
            P("tp", None),
            P("tp", None),
        ),
        out_specs=P(("sp", "tp"), None),
        check_vma=False,
    )
```

profile of v0, /device:TPU:27, one launch (start us, length us, event | category | flops | bytes accessed | tf_op | source)
XLA Modules:
  0.0 305.2 jit_solution(18365934539425625219)
XLA Ops:
  6.5 0.7 all-gather.4.cloned.1.call-update
  7.3 0.7 collective-permute-start.1
  8.6 0.8 slice.117
  9.4 0.8 slice.118
  10.3 3.1 %collective-permute-start = (bf16[128,512]{1,0:T(8,128)(2,1)S(1)}, bf16[128,512]{1,0:T(8,128)(2,1)S(1)}, u32[]{:S(2)}, u32[]{:S(2)}) collective-permute-start(bf16[128,512]{1,0:T(8,128)(2,1)S(1)} %pad_maximum_fusion.6), channel_id=1, source_target_pairs={{0,8},{8,16},{16,24},{1,9},{9,17},{17,25},{2,10},{10,18},{18,26},{... | collective-permute-start | bytes 393224 | tf_op jit(solution)/shard_map/ppermute | solution.py:16
  13.4 1.2 constant_dynamic-slice_fusion
  16.2 0.9 collective-permute-done
  18.8 20.7 %all_to_all.39 = bf16[8,128,128]{1,2,0:T(8,128)(2,1)S(1)} all-to-all(bf16[8,128,128]{1,2,0:T(8,128)(2,1)S(1)} %bitcast.88), channel_id=1, replica_groups=mesh['sp'=4,'tp'=8] {'tp'}, dimensions={0} | all-to-all | bytes 524288 | tf_op jit(solution)/shard_map/all_to_all | solution.py:115
  39.5 21.1 %all-gather.4.cloned.1.call-done = bf16[1024,2048]{1,0:T(8,128)(2,1)} async-done(((bf16[128,2048]{1,0:T(8,128)(2,1)}), bf16[1024,2048]{1,0:T(8,128)(2,1)}) %all-gather.4.cloned.1.call-update) | async-done | bytes 4194320 | tf_op jit(solution)/shard_map/all_gather | solution.py:121
  60.7 3.0 multiply_reduce_fusion
  63.9 0.8 fusion.64
  64.8 0.7 all-gather.6.cloned.1.call-update
  66.7 26.8 %all-gather.8.cloned.1.call-done = bf16[1024,1024]{1,0:T(8,128)(2,1)} async-done(((bf16[128,1024]{1,0:T(8,128)(2,1)}), bf16[1024,1024]{1,0:T(8,128)(2,1)}) %all-gather.8.cloned.1.call-update) | async-done | bytes 2097168 | tf_op jit(solution)/shard_map/all_gather | solution.py:142
  93.4 5.2 %convolution_convert_fusion = bf16[1024,1024]{1,0:T(8,128)(2,1)} fusion(bf16[1024,1024]{1,0:T(8,128)(2,1)} %all-gather.8.cloned.1.call-done, bf16[256,1024]{1,0:T(8,128)(2,1)S(1)} %get-tuple-element.45, bf16[256,1024]{1,0:T(8,128)(2,1)S(1)} %get-tuple-element.46, bf16[256,1024]{1,0:T(8,128)(2,1)S(1)} %get-tuple-element.47, ...), kind=kOutput, calls=%fused_computation.19 | convolution fusion | flops 2156920832 | bytes 6291456 | tf_op jit(solution)/shard_map/dot_general | solution.py:143
  98.7 3.9 %all-to-all-start.2 = ((bf16[4,256,1024]{2,1,0:T(8,128)(2,1)}), bf16[4,256,1024]{2,1,0:T(8,128)(2,1)S(1)}, u32[]{:S(2)}, u32[]{:S(2)}) async-start(bf16[4,256,1024]{2,1,0:T(8,128)(2,1)} %bitcast.78), calls=%async_computation.2 | async-start | bytes 4194304 | tf_op jit(solution)/shard_map/all_to_all | solution.py:144
  103.2 1.6 select_convert_fusion.4
  104.8 18.8 %all-gather.6.cloned.1.call-done = bf16[1024,1024]{1,0:T(8,128)(2,1)} async-done(((bf16[128,1024]{1,0:T(8,128)(2,1)}), bf16[1024,1024]{1,0:T(8,128)(2,1)}) %all-gather.6.cloned.1.call-update) | async-done | bytes 2097168 | tf_op jit(solution)/shard_map/all_gather | solution.py:142
  123.6 5.9 %convolution_convert_fusion.1 = bf16[1024,1024]{1,0:T(8,128)(2,1)} fusion(bf16[1024,1024]{1,0:T(8,128)(2,1)} %all-gather.6.cloned.1.call-done, bf16[256,1024]{1,0:T(8,128)(2,1)} %copy-done.13, bf16[256,1024]{1,0:T(8,128)(2,1)} %copy-done.14, bf16[256,1024]{1,0:T(8,128)(2,1)} %copy-done.15, bf16[256,1024]{1,0:T(8,128)(2,1)} %copy-done.16), kind=kOutput, calls=%fused_computation.20 | convolution fusion | flops 2156920832 | bytes 6291456 | tf_op jit(solution)/shard_map/dot_general | solution.py:143
  129.5 1.4 copy-done.3
  130.9 4.8 %all-to-all-start.1 = ((bf16[4,256,1024]{2,1,0:T(8,128)(2,1)}), bf16[4,256,1024]{2,1,0:T(8,128)(2,1)}, u32[]{:S(2)}, u32[]{:S(2)}) async-start(bf16[4,256,1024]{2,1,0:T(8,128)(2,1)} %bitcast.79), calls=%async_computation.1 | async-start | bytes 4194304 | tf_op jit(solution)/shard_map/all_to_all | solution.py:144
  135.7 1.6 select_convert_fusion.6
  137.4 0.8 fusion.50
  138.1 1.5 convolution_add_fusion.2
  139.6 4.8 %fusion.13 = f32[1024,768]{1,0:T(8,128)} fusion(bf16[1024,1024]{1,0:T(8,128)(2,1)S(1)} %bitcast.74, bf16[768,2048]{1,0:T(8,128)(2,1)} %bitcast.105), kind=kOutput, calls=%fused_computation.28 | convolution fusion | flops 1610612736 | bytes 6815744 | tf_op jit(solution)/shard_map/td,fd->tf/dot_general | solution.py:149
  144.5 4.9 %fusion.22 = f32[1024,768]{1,0:T(8,128)} fusion(bf16[1024,1024]{1,0:T(8,128)(2,1)S(1)} %bitcast.75, bf16[768,2048]{1,0:T(8,128)(2,1)} %collective-permute-done.1), kind=kOutput, calls=%fused_computation.37 | convolution fusion | flops 1610612736 | bytes 6815744 | tf_op jit(solution)/shard_map/td,fd->tf/dot_general | solution.py:149
  149.3 10.9 %all-to-all-done.1 = bf16[4,256,1024]{2,1,0:T(8,128)(2,1)} async-done(((bf16[4,256,1024]{2,1,0:T(8,128)(2,1)}), bf16[4,256,1024]{2,1,0:T(8,128)(2,1)}, u32[]{:S(2)}, u32[]{:S(2)}) %all-to-all-start.1) | async-done | bytes 2097184 | tf_op jit(solution)/shard_map/all_to_all | solution.py:144
  160.2 4.0 %fusion.24 = f32[1024,768]{1,0:T(8,128)S(1)} fusion(bf16[1024,1024]{1,0:T(8,128)(2,1)} %bitcast.32, bf16[768,2048]{1,0:T(8,128)(2,1)} %collective-permute-done.1), kind=kOutput, calls=%fused_computation.39 | convolution fusion | flops 1610612736 | bytes 6815744 | tf_op jit(solution)/shard_map/td,fd->tf/dot_general | solution.py:149
  164.3 3.6 %fusion.11 = f32[1024,768]{1,0:T(8,128)S(1)} fusion(bf16[1024,1024]{1,0:T(8,128)(2,1)} %bitcast.32, bf16[768,2048]{1,0:T(8,128)(2,1)S(1)} %bitcast.108), kind=kOutput, calls=%fused_computation.26 | convolution fusion | flops 1610612736 | bytes 6815744 | tf_op jit(solution)/shard_map/td,fd->tf/dot_general | solution.py:149
  167.9 3.6 %fusion.15 = f32[1024,768]{1,0:T(8,128)S(1)} fusion(bf16[1024,1024]{1,0:T(8,128)(2,1)} %bitcast.32, bf16[768,2048]{1,0:T(8,128)(2,1)S(1)} %bitcast.106), kind=kOutput, calls=%fused_computation.30 | convolution fusion | flops 1610612736 | bytes 6815744 | tf_op jit(solution)/shard_map/td,fd->tf/dot_general | solution.py:149
  171.5 3.4 %fusion.19 = f32[1024,768]{1,0:T(8,128)S(1)} fusion(bf16[1024,1024]{1,0:T(8,128)(2,1)S(1)} %bitcast.76, bf16[768,2048]{1,0:T(8,128)(2,1)} %collective-permute-done.2), kind=kOutput, calls=%fused_computation.34 | convolution fusion | flops 1610612736 | bytes 6815744 | tf_op jit(solution)/shard_map/td,fd->tf/dot_general | solution.py:149
  174.9 2.3 multiply_convert_fusion.1
  177.2 2.0 fusion.8
  179.6 4.3 %multiply_convert_fusion = bf16[1024,768]{1,0:T(8,128)(2,1)S(1)} fusion(f32[1024,768]{1,0:T(8,128)S(1)} %fusion.19, f32[1024,768]{1,0:T(8,128)S(1)} %fusion.24, f32[1024,768]{1,0:T(8,128)S(1)} %copy-done.30, bf16[1024,1024]{1,0:T(8,128)(2,1)} %bitcast.32, bf16[768,2048]{1,0:T(8,128)(2,1)} %collective-permute-done.2), kind=kOutput, calls=%fused_computation.7 | convolution fusion | flops 1616904192 | bytes 14680064 | tf_op jit(solution)/shard_map/td,fd->tf/dot_general | solution.py:149
  184.0 5.1 %add_convert_fusion.3 = bf16[1024,1024]{1,0:T(8,128)(2,1)} fusion(f32[1024,1024]{1,0:T(8,128)S(1)} %fusion.8, bf16[1024,768]{1,0:T(8,128)(2,1)S(1)} %multiply_convert_fusion, bf16[768,2048]{1,0:T(8,128)(2,1)} %collective-permute-done.3), kind=kOutput, calls=%fused_computation.3 | convolution fusion | flops 1612709888 | bytes 9437184 | tf_op jit(solution)/shard_map/dot_general | solution.py:163
  189.1 4.7 %all-to-all-start.3 = ((bf16[4,256,1024]{2,1,0:T(8,128)(2,1)}), bf16[4,256,1024]{2,1,0:T(8,128)(2,1)}, u32[]{:S(2)}, u32[]{:S(2)}) async-start(bf16[4,256,1024]{2,1,0:T(8,128)(2,1)} %bitcast.81), calls=%async_computation.3 | async-start | bytes 4194304 | tf_op jit(solution)/shard_map/all_to_all | solution.py:168
  193.9 1.8 fusion.47
  195.7 1.8 fusion.27
  197.6 3.3 %fusion.6 = f32[1024,1024]{1,0:T(8,128)S(1)} fusion(bf16[1024,768]{1,0:T(8,128)(2,1)} %copy-done.29, bf16[768,2048]{1,0:T(8,128)(2,1)S(1)} %bitcast.112), kind=kOutput, calls=%fused_computation.21 | convolution fusion | flops 1610612736 | bytes 7340032 | tf_op jit(solution)/shard_map/dot_general | solution.py:163
  201.0 3.2 %add_convert_fusion.2 = bf16[1024,1024]{1,0:T(8,128)(2,1)S(1)} fusion(f32[1024,1024]{1,0:T(8,128)S(1)} %fusion.6, bf16[1024,768]{1,0:T(8,128)(2,1)S(1)} %copy-done.33, bf16[768,2048]{1,0:T(8,128)(2,1)} %collective-permute-done.3), kind=kOutput, calls=%fused_computation.2 | convolution fusion | flops 1612709888 | bytes 9437184 | tf_op jit(solution)/shard_map/dot_general | solution.py:163
  204.2 13.2 %all-to-all-done.3 = bf16[4,256,1024]{2,1,0:T(8,128)(2,1)} async-done(((bf16[4,256,1024]{2,1,0:T(8,128)(2,1)}), bf16[4,256,1024]{2,1,0:T(8,128)(2,1)}, u32[]{:S(2)}, u32[]{:S(2)}) %all-to-all-start.3) | async-done | bytes 2097184 | tf_op jit(solution)/shard_map/all_to_all | solution.py:168
  217.5 4.6 %fusion.35 = f32[1024,1024]{1,0:T(8,128)S(1)} fusion(bf16[1024,1024]{1,0:T(8,128)(2,1)} %bitcast.37, bf16[1024,256]{1,0:T(8,128)(2,1)} %get-tuple-element.49, bf16[1024,256]{1,0:T(8,128)(2,1)} %get-tuple-element.50, bf16[1024,256]{1,0:T(8,128)(2,1)} %get-tuple-element.51, bf16[1024,256]{1,0:T(8,128)(2,1)} %get-tuple-element.52), kind=kOutput, calls=%fused_computation.72 | convolution fusion | flops 2155872256 | bytes 8388608 | tf_op jit(solution)/shard_map/dot_general | solution.py:173
  222.1 2.1 add_convert_fusion.1
  224.3 26.4 %all_to_all.40 = bf16[4,256,1024]{2,1,0:T(8,128)(2,1)S(1)} all-to-all(bf16[4,256,1024]{2,1,0:T(8,128)(2,1)S(1)} %bitcast.80), channel_id=1, replica_groups=mesh['sp'=4,'tp'=8] {'sp'}, dimensions={0} | all-to-all | bytes 4194304 | tf_op jit(solution)/shard_map/all_to_all | solution.py:168
  250.6 2.3 fusion.34
  253.0 2.1 add_convert_fusion
  255.1 5.0 %reduce-scatter.3.cloned.1.call-done = bf16[128,1024]{1,0:T(8,128)(2,1)} async-done(((bf16[1024,1024]{1,0:T(8,128)(2,1)}), bf16[128,1024]{1,0:T(8,128)(2,1)}) %reduce-scatter.3.cloned.1.call-update) | async-done | bytes 262160 | tf_op jit(solution)/shard_map/reduce_scatter | solution.py:175
  260.1 36.6 %reduce-scatter.5.cloned.1.call-done = bf16[128,1024]{1,0:T(8,128)(2,1)} async-done(((bf16[1024,1024]{1,0:T(8,128)(2,1)}), bf16[128,1024]{1,0:T(8,128)(2,1)}) %reduce-scatter.5.cloned.1.call-update) | async-done | bytes 262160 | tf_op jit(solution)/shard_map/reduce_scatter | solution.py:175
  296.7 1.9 add_convert_fusion.4
  (113 shorter events, 6.4 us)
Async XLA Ops:
  6.5 8.4 %copy-start.6 = (bf16[1024,256]{1,0:T(8,128)(2,1)S(1)}, bf16[1024,256]{1,0:T(8,128)(2,1)}, u32[]{:S(2)}) copy-start(bf16[1024,256]{1,0:T(8,128)(2,1)} %param.16) | copy-start | bytes 1572868
  6.5 8.4 %copy-start.7 = (bf16[1024,256]{1,0:T(8,128)(2,1)S(1)}, bf16[1024,256]{1,0:T(8,128)(2,1)}, u32[]{:S(2)}) copy-start(bf16[1024,256]{1,0:T(8,128)(2,1)} %param.17) | copy-start | bytes 1572868
  6.5 54.1 %all-gather.4.cloned.1.call-start = ((), (), s32[]{:S(2)}) async-start(), calls=%async_computation.7 | async-start | bytes 4718592 | tf_op jit(solution)/shard_map/all_gather | solution.py:121
  7.3 8.2 %copy-start.17 = (bf16[1024,128]{1,0:T(8,128)(2,1)S(1)}, bf16[1024,128]{1,0:T(8,128)(2,1)}, u32[]{:S(2)}) copy-start(bf16[1024,128]{1,0:T(8,128)(2,1)} %param.15) | copy-start | bytes 786436
  7.3 86.1 %all-gather.8.cloned.1.call-start = ((), (), s32[]{:S(2)}) async-start(), calls=%async_computation.9 | async-start | bytes 2359296 | tf_op jit(solution)/shard_map/all_gather | solution.py:142
  7.3 32.2 %collective-permute-start.1 = (bf16[768,2048]{1,0:T(8,128)(2,1)}, bf16[768,2048]{1,0:T(8,128)(2,1)}, u32[]{:S(2)}, u32[]{:S(2)}) collective-permute-start(bf16[768,2048]{1,0:T(8,128)(2,1)} %bitcast.104), channel_id=1, source_target_pairs={{0,1},{1,0},{2,3},{3,2},{4,5},{5,4},{6,7},{7,6},{8,9},{9,8},{10,11... | collective-permute-start | bytes 9437192 | tf_op jit(solution)/shard_map/ppermute | solution.py:20
  8.1 31.4 %collective-permute-start.2 = (bf16[768,2048]{1,0:T(8,128)(2,1)}, bf16[768,2048]{1,0:T(8,128)(2,1)}, u32[]{:S(2)}, u32[]{:S(2)}) collective-permute-start(bf16[768,2048]{1,0:T(8,128)(2,1)} %bitcast.107), channel_id=1, source_target_pairs={{0,1},{1,0},{2,3},{3,2},{4,5},{5,4},{6,7},{7,6},{8,9},{9,8},{10,11... | collective-permute-start | bytes 9437192 | tf_op jit(solution)/shard_map/ppermute | solution.py:20
  8.1 31.4 %collective-permute-start.3 = (bf16[768,2048]{1,0:T(8,128)(2,1)}, bf16[768,2048]{1,0:T(8,128)(2,1)}, u32[]{:S(2)}, u32[]{:S(2)}) collective-permute-start(bf16[768,2048]{1,0:T(8,128)(2,1)} %bitcast.110), channel_id=1, source_target_pairs={{0,1},{1,0},{2,3},{3,2},{4,5},{5,4},{6,7},{7,6},{8,9},{9,8},{10,11... | collective-permute-start | bytes 9437192 | tf_op jit(solution)/shard_map/ppermute | solution.py:20
  10.3 6.9 %collective-permute-start = (bf16[128,512]{1,0:T(8,128)(2,1)S(1)}, bf16[128,512]{1,0:T(8,128)(2,1)S(1)}, u32[]{:S(2)}, u32[]{:S(2)}) collective-permute-start(bf16[128,512]{1,0:T(8,128)(2,1)S(1)} %pad_maximum_fusion.6), channel_id=1, source_target_pairs={{0,8},{8,16},{16,24},{1,9},{9,17},{17,25},{2,10},{10,18},{18,26},{... | collective-permute-start | bytes 393224 | tf_op jit(solution)/shard_map/ppermute | solution.py:16
  15.9 2.1 copy-start.24
  18.5 42.2 %copy-start.8 = (bf16[128,2048]{1,0:T(8,128)(2,1)S(1)}, bf16[128,2048]{1,0:T(8,128)(2,1)}, u32[]{:S(2)}) copy-start(bf16[128,2048]{1,0:T(8,128)(2,1)} %param.20) | copy-start | bytes 1572868
  39.5 24.2 %copy-start.23 = (f32[2048]{0:T(1024)S(1)}, f32[2048]{0:T(1024)}, u32[]{:S(2)}) copy-start(f32[2048]{0:T(1024)} %param.21) | copy-start | bytes 24580
  63.7 1.8 copy-start.21
  64.7 58.9 %all-gather.6.cloned.1.call-start = ((), (), s32[]{:S(2)}) async-start(), calls=%async_computation.8 | async-start | bytes 2359296 | tf_op jit(solution)/shard_map/all_gather | solution.py:142
  66.4 32.3 %copy-start.13 = (bf16[256,1024]{1,0:T(8,128)(2,1)}, bf16[256,1024]{1,0:T(8,128)(2,1)S(1)}, u32[]{:S(2)}) copy-start(bf16[256,1024]{1,0:T(8,128)(2,1)S(1)} %get-tuple-element.45) | copy-start | bytes 1572868
  66.4 32.3 %copy-start.14 = (bf16[256,1024]{1,0:T(8,128)(2,1)}, bf16[256,1024]{1,0:T(8,128)(2,1)S(1)}, u32[]{:S(2)}) copy-start(bf16[256,1024]{1,0:T(8,128)(2,1)S(1)} %get-tuple-element.46) | copy-start | bytes 1572868
  66.6 32.0 %copy-start.15 = (bf16[256,1024]{1,0:T(8,128)(2,1)}, bf16[256,1024]{1,0:T(8,128)(2,1)S(1)}, u32[]{:S(2)}) copy-start(bf16[256,1024]{1,0:T(8,128)(2,1)S(1)} %get-tuple-element.47) | copy-start | bytes 1572868
  66.6 32.0 %copy-start.16 = (bf16[256,1024]{1,0:T(8,128)(2,1)}, bf16[256,1024]{1,0:T(8,128)(2,1)S(1)}, u32[]{:S(2)}) copy-start(bf16[256,1024]{1,0:T(8,128)(2,1)S(1)} %get-tuple-element.48) | copy-start | bytes 1572868
  98.7 3.9 %copy-start.22 = (f32[1024,4]{0,1:T(4,128)S(1)}, f32[1024,4]{0,1:T(4,128)}, u32[]{:S(2)}) copy-start(f32[1024,4]{0,1:T(4,128)} %param.23) | copy-start | bytes 49156
  98.7 30.8 %all-to-all-start.2 = ((bf16[4,256,1024]{2,1,0:T(8,128)(2,1)}), bf16[4,256,1024]{2,1,0:T(8,128)(2,1)S(1)}, u32[]{:S(2)}, u32[]{:S(2)}) async-start(bf16[4,256,1024]{2,1,0:T(8,128)(2,1)} %bitcast.78), calls=%async_computation.2 | async-start | bytes 4194304 | tf_op jit(solution)/shard_map/all_to_all | solution.py:144
  129.5 1.4 copy-start.3
  130.9 6.4 %copy-start = (bf16[1024,1024]{1,0:T(8,128)(2,1)S(1)}, bf16[1024,1024]{1,0:T(8,128)(2,1)}, u32[]{:S(2)}) copy-start(bf16[1024,1024]{1,0:T(8,128)(2,1)} %all-gather.6.cloned.1.call-done) | copy-start | bytes 6291460
  130.9 6.4 %copy-start.19 = (bf16[64,2048]{1,0:T(8,128)(2,1)S(1)}, bf16[64,2048]{1,0:T(8,128)(2,1)}, u32[]{:S(2)}) copy-start(bf16[64,2048]{1,0:T(8,128)(2,1)} %param.27) | copy-start | bytes 786436
  130.9 29.3 %all-to-all-start.1 = ((bf16[4,256,1024]{2,1,0:T(8,128)(2,1)}), bf16[4,256,1024]{2,1,0:T(8,128)(2,1)}, u32[]{:S(2)}, u32[]{:S(2)}) async-start(bf16[4,256,1024]{2,1,0:T(8,128)(2,1)} %bitcast.79), calls=%async_computation.1 | async-start | bytes 4194304 | tf_op jit(solution)/shard_map/all_to_all | solution.py:144
  135.7 2.4 copy-start.1
  137.4 2.3 copy-start.4
  160.2 4.0 %copy-start.26 = (bf16[1,768,2048]{2,1,0:T(8,128)(2,1)S(1)}, bf16[1,768,2048]{2,1,0:T(8,128)(2,1)}, u32[]{:S(2)}) copy-start(bf16[1,768,2048]{2,1,0:T(8,128)(2,1)} %param.25) | copy-start | bytes 9437188
  164.2 3.6 %copy-start.25 = (bf16[1,768,2048]{2,1,0:T(8,128)(2,1)S(1)}, bf16[1,768,2048]{2,1,0:T(8,128)(2,1)}, u32[]{:S(2)}) copy-start(bf16[1,768,2048]{2,1,0:T(8,128)(2,1)} %param.24) | copy-start | bytes 9437188
  167.8 3.6 %copy-start.5 = (bf16[4,256,1024]{2,1,0:T(8,128)(2,1)S(1)}, bf16[4,256,1024]{2,1,0:T(8,128)(2,1)}, u32[]{:S(2)}) copy-start(bf16[4,256,1024]{2,1,0:T(8,128)(2,1)} %copy-done.3) | copy-start | bytes 6291460
  171.4 3.4 %copy-start.31 = (f32[1024,768]{1,0:T(8,128)S(1)}, f32[1024,768]{1,0:T(8,128)}, u32[]{:S(2)}) copy-start(f32[1024,768]{1,0:T(8,128)} %fusion.13) | copy-start | bytes 9437188
  174.9 2.3 copy-start.27
  177.2 2.0 copy-start.29
  177.2 2.5 copy-start.30
  184.0 5.1 %copy-start.32 = (bf16[1024,768]{1,0:T(8,128)(2,1)}, bf16[1024,768]{1,0:T(8,128)(2,1)S(1)}, u32[]{:S(2)}) copy-start(bf16[1024,768]{1,0:T(8,128)(2,1)S(1)} %multiply_convert_fusion) | copy-start | bytes 4718596
  189.1 28.3 %all-to-all-start.3 = ((bf16[4,256,1024]{2,1,0:T(8,128)(2,1)}), bf16[4,256,1024]{2,1,0:T(8,128)(2,1)}, u32[]{:S(2)}, u32[]{:S(2)}) async-start(bf16[4,256,1024]{2,1,0:T(8,128)(2,1)} %bitcast.81), calls=%async_computation.3 | async-start | bytes 4194304 | tf_op jit(solution)/shard_map/all_to_all | solution.py:168
  193.9 1.8 copy-start.20
  193.9 66.2 %reduce-scatter.3.cloned.1.call-start = ((), (), s32[]{:S(2)}) async-start(), calls=%async_computation.10 | async-start | bytes 2359296 | tf_op jit(solution)/shard_map/reduce_scatter | solution.py:175
  193.9 1.8 copy-start.2
  195.7 2.0 copy-start.28
  197.6 3.3 %copy-start.33 = (bf16[1024,768]{1,0:T(8,128)(2,1)S(1)}, bf16[1024,768]{1,0:T(8,128)(2,1)}, u32[]{:S(2)}) copy-start(bf16[1024,768]{1,0:T(8,128)(2,1)} %copy-done.32) | copy-start | bytes 4718596
  217.5 4.6 %copy-start.18 = (bf16[64,2048]{1,0:T(8,128)(2,1)S(1)}, bf16[64,2048]{1,0:T(8,128)(2,1)}, u32[]{:S(2)}) copy-start(bf16[64,2048]{1,0:T(8,128)(2,1)} %param.29) | copy-start | bytes 786436
  224.2 72.5 %reduce-scatter.5.cloned.1.call-start = ((), (), s32[]{:S(2)}) async-start(), calls=%async_computation.11 | async-start | bytes 2359296 | tf_op jit(solution)/shard_map/reduce_scatter | solution.py:175
  224.2 26.4 %copy-start.9 = (bf16[1024,256]{1,0:T(8,128)(2,1)S(1)}, bf16[1024,256]{1,0:T(8,128)(2,1)}, u32[]{:S(2)}) copy-start(bf16[1024,256]{1,0:T(8,128)(2,1)} %get-tuple-element.49) | copy-start | bytes 1572868
  224.2 26.4 %copy-start.10 = (bf16[1024,256]{1,0:T(8,128)(2,1)S(1)}, bf16[1024,256]{1,0:T(8,128)(2,1)}, u32[]{:S(2)}) copy-start(bf16[1024,256]{1,0:T(8,128)(2,1)} %get-tuple-element.50) | copy-start | bytes 1572868
  224.3 26.4 %copy-start.11 = (bf16[1024,256]{1,0:T(8,128)(2,1)S(1)}, bf16[1024,256]{1,0:T(8,128)(2,1)}, u32[]{:S(2)}) copy-start(bf16[1024,256]{1,0:T(8,128)(2,1)} %get-tuple-element.51) | copy-start | bytes 1572868
  224.3 26.4 %copy-start.12 = (bf16[1024,256]{1,0:T(8,128)(2,1)S(1)}, bf16[1024,256]{1,0:T(8,128)(2,1)}, u32[]{:S(2)}) copy-start(bf16[1024,256]{1,0:T(8,128)(2,1)} %get-tuple-element.52) | copy-start | bytes 1572868
Sparse Core Ops, SparseCore 0:
  8.9 51.6 all-gather.3
  64.8 28.5 all-gather.7
  95.0 28.5 all-gather.5
  224.3 35.7 reduce-scatter.2
  262.2 34.4 reduce-scatter.4
where the time goes:
time: 310 us; the launch traced here: 305 us
  waiting for transfers between devices  135 us (44%)
  matrix products  77.5 us (25%)
  blocking collectives  47 us (15%)
  starting transfers between devices  17.9 us (6%)
  between operations  13.8 us (4%)
  local copies, waits for them, and re-layouts  7.28 us (2%)
  other arithmetic  6.92 us (2%)
    all_gather x2, waiting for transfers between devices, body(): rows = lax.all_gather(normed[:, cols], 'tp', axis=0, tiled=True)  45.6 us
    reduce_scatter x2, waiting for transfers between devices, body(): lax.psum_scatter(part.astype(jnp.bfloat16), 'tp', scatter_dimension=0, ti...  41.7 us
    dot_general x8, matrix products, body(): jnp.einsum('td,fd->tf', arrived, w[:, cols], preferred_element_type=jnp.f...  30.9 us
    all_to_all x1, blocking collectives, body(): lax.all_to_all(outs[c], 'sp', split_axis=0, concat_axis=0, tiled=True)  26.4 us
    all_gather x1, waiting for transfers between devices, body(): lax.all_gather(w_out, 'tp', axis=0, tiled=True)  21.1 us
    all_to_all x1, blocking collectives, body(): lax.all_to_all(attended, 'tp', split_axis=0, concat_axis=1, tiled=True)  20.7 us
    dot_general x4, matrix products, body(): jnp.dot(h, w[:, cols], preferred_element_type=jnp.float32)  13.7 us
    all_to_all x1, waiting for transfers between devices, body(): lax.all_to_all(outs[c], 'sp', split_axis=0, concat_axis=0, tiled=True)  13.2 us
  transfers between devices with their start and end apart: 12, of which 8 were waited for; matrix products, arithmetic and copies ran while one was open for 16% of the time, Pallas kernels for 0%

commit v1 on v0

v1 whole, which is shorter than its diff:
```python
import functools

import jax
import jax.numpy as jnp
from jax import lax
from jax.experimental import pallas as pl
from jax.experimental.pallas import tpu as pltpu
from jax.sharding import PartitionSpec as P

HD = 64
GROUP = 4
WINDOW = 128
TOPK = 4
CHUNKS = 4
TILE = 256
MESH = pl.DeviceIdType.MESH
F32 = jnp.float32
BF16 = jnp.bfloat16
NT = (((1,), (1,)), ((), ()))


def dot(a, b):
    return jnp.dot(a, b, preferred_element_type=F32)


def dot_t(a, b):
    return lax.dot_general(a, b, NT, preferred_element_type=F32)


def silu(v):
    return v / (1.0 + jnp.exp(jnp.minimum(-v, 87.0)))


def loop(n, body):
    lax.fori_loop(0, n, lambda i, carry: (body(i), carry)[1], 0)


def moe_kernel(
    normed,
    after_mix,
    place_t,
    place,
    weight,
    w_gate,
    w_up,
    w_down,
    s_gate,
    s_up,
    s_down,
    out,
    wg,
    wu,
    wd,
    sgu,
    sd,
    gathered,
    onehot,
    mix,
    sent,
    arrived,
    acc_g,
    acc_u,
    sh_acc,
    sh,
    returned,
    x_recv,
    z_recv,
    w_sem,
    pw_send,
    pw_recv,
    s_sem,
    ag_send,
    ag_recv,
    fw_send,
    fw_recv,
    d_send,
    d_recv,
    r_send,
    r_recv,
    x_ssem,
    x_rsem,
    z_ssem,
    z_rsem,
):
    n_sp = lax.axis_size("sp")
    n_tp = lax.axis_size("tp")
    lanes = n_tp // 2
    s = lax.axis_index("sp")
    t = lax.axis_index("tp")
    z = t // 2
    core = t % 2
    rows = normed.shape[0]
    chunks, _, _, step = gathered.shape
    half_cap = sent.shape[2]
    slots = n_sp * half_cap
    ff = wg.shape[1] // 2
    sff = sd.shape[1]
    bands = 2 * ff // TILE
    per = step // TILE

    def sp_peer(j):
        return {"sp": (s + j) % n_sp}

    def z_peer(j):
        return {"tp": ((z + j) % lanes) * 2 + core}

    partner = {"tp": z * 2 + 1 - core}

    barrier = pltpu.get_barrier_semaphore()
    for j in range(1, n_sp):
        pl.semaphore_signal(barrier, inc=1, device_id=sp_peer(j), device_id_type=MESH)
    for j in range(1, lanes):
        pl.semaphore_signal(barrier, inc=1, device_id=z_peer(j), device_id_type=MESH)
    pl.semaphore_signal(barrier, inc=1, device_id=partner, device_id_type=MESH)
    pl.semaphore_wait(barrier, n_sp - 1 + lanes - 1 + 1)

    def cols(c):
        return pl.ds(pl.multiple_of(c * step, step), step)

    def remote(src, dst, send, recv, peer):
        return pltpu.make_async_remote_copy(
            src_ref=src, dst_ref=dst, send_sem=send, recv_sem=recv, device_id=peer, device_id_type=MESH
        )

    def own_piece(c, j):
        return remote(normed.at[:, cols(c)], gathered.at[c, t], ag_send.at[c, j], ag_recv.at[c, j], z_peer(j))

    def own_to_partner(c):
        return remote(normed.at[:, cols(c)], gathered.at[c, t], fw_send.at[c, 0], fw_recv.at[c, 0], partner)

    def forward(c, j):
        src = gathered.at[c, ((z + lanes - j) % lanes) * 2 + core]
        return remote(src, src, fw_send.at[c, j], fw_recv.at[c, j], partner)

    def dispatch(c, j):
        return remote(sent.at[c, j], arrived.at[c, j], d_send.at[c, j], d_recv.at[c, j], sp_peer(j))

    def give_back(c, j):
        return remote(
            sent.at[c, j], returned.at[c, j], r_send.at[c, j], r_recv.at[c, j], sp_peer(n_sp - j)
        )

    def cross(c):
        return remote(gathered.at[c, 0:lanes], x_recv.at[c], x_ssem.at[c], x_rsem.at[c], partner)

    def spread(c, j):
        return remote(gathered.at[c, lanes + j], z_recv.at[c, j], z_ssem.at[c, j], z_rsem.at[c, j], z_peer(j))

    weights = ((w_gate, wg), (w_up, wu), (w_down, wd))
    shared = (
        (s_gate, lambda c: sgu.at[c, 0:sff]),
        (s_up, lambda c: sgu.at[c, sff : 2 * sff]),
        (s_down, lambda c: sd.at[c]),
    )

    def own_weight(n, c):
        src, dst = weights[n]
        return pltpu.make_async_copy(src.at[0, :, cols(c)], dst.at[c, 0:ff], w_sem.at[n, c])

    def other_weight(n, c):
        src, dst = weights[n]
        return remote(src.at[0, :, cols(c)], dst.at[c, ff : 2 * ff], pw_send.at[n, c], pw_recv.at[n, c], partner)

    def shared_weight(n, c):
        src, dst = shared[n]
        return pltpu.make_async_copy(src.at[:, cols(c)], dst(c), s_sem.at[n, c])

    def start_sends(c):
        for j in range(1, lanes):
            own_piece(c, j).start()
        own_to_partner(c).start()

    loop(chunks, start_sends)

    def start_weights(c):
        for n in range(2):
            own_weight(n, c).start()
            other_weight(n, c).start()
            shared_weight(n, c).start()

    loop(chunks, start_weights)

    def start_down(c):
        own_weight(2, c).start()
        other_weight(2, c).start()
        shared_weight(2, c).start()

    loop(chunks, start_down)

    def keep_own(c):
        gathered[c, t] = normed[:, cols(c)]

    loop(chunks, keep_own)

    slot_down = lax.broadcasted_iota(jnp.int32, (half_cap, 1), 0).astype(F32)
    slot_along = lax.broadcasted_iota(jnp.int32, (1, half_cap), 1).astype(F32)

    def build_pick(j):
        hit = place_t[j] == slot_down
        onehot[j] = jnp.where(hit, 1.0, 0.0).astype(BF16)

    loop(n_sp, build_pick)

    def build_mix(i):
        for j in range(n_sp):
            hit = place[i, :, j : j + 1] == slot_along
            part = jnp.where(hit, weight[i, :, j : j + 1], 0.0).astype(BF16)
            mix[i, :, j * half_cap : (j + 1) * half_cap] = part

    loop(n_tp, build_mix)

    def gather_chunk(c):
        for j in range(1, lanes):
            own_piece(c, j).wait_recv()
            forward(c, j).start()
        own_to_partner(c).wait_recv()
        for j in range(1, lanes):
            forward(c, j).wait_recv()

    def pick_chunk(c):
        block = gathered[c].reshape(n_tp * rows, step)

        def one(i):
            j = (i + 1) % n_sp
            value = dot(onehot[j], block).astype(BF16)

            @pl.when(j > 0)
            def _():
                sent[c, j] = value
                dispatch(c, j).start()

            @pl.when(j == 0)
            def _():
                arrived[c, j] = value

        loop(n_sp, one)

    def shared_chunk(c):
        for n in range(2):
            shared_weight(n, c).wait()
        block = gathered[c].reshape(n_tp * rows, step)
        value = dot_t(block, sgu[c])

        @pl.when(c == 0)
        def _():
            sh_acc[...] = value

        @pl.when(c > 0)
        def _():
            sh_acc[...] += value

    def expert_chunk(c):
        for n in range(2):
            own_weight(n, c).wait()
            other_weight(n, c).wait_recv()

        for j in range(1, n_sp):
            dispatch(c, j).wait_recv()
        lhs = arrived[c].reshape(slots, step)

        def one(i):
            band = pl.ds(pl.multiple_of(i * TILE, TILE), TILE)
            for w, acc in ((wg, acc_g), (wu, acc_u)):
                value = dot_t(lhs, w[c, band, :])

                @pl.when(c == 0)
                def _():
                    acc[i] = value

                @pl.when(c > 0)
                def _():
                    acc[i] += value

        loop(bands, one)

    def dispatch_step(c):
        gather_chunk(c)
        pick_chunk(c)
        shared_chunk(c)

        @pl.when(c > 0)
        def _():
            expert_chunk(c - 1)

    loop(chunks, dispatch_step)
    expert_chunk(chunks - 1)

    def activate(i):
        value = (silu(acc_g[i]) * acc_u[i]).astype(BF16).reshape(n_sp, half_cap, TILE)
        band = pl.ds(pl.multiple_of(i % per * TILE, TILE), TILE)
        arrived[i // per, :, :, band] = value

    loop(bands, activate)
    shared_value = silu(sh_acc[:, 0:sff]) * sh_acc[:, sff : 2 * sff]
    sh[...] = shared_value.astype(BF16).reshape(sh.shape)

    def settle_dispatch(c):
        for j in range(1, n_sp):
            dispatch(c, j).wait_send()
        for j in range(1, lanes):
            forward(c, j).wait_send()

    loop(chunks, settle_dispatch)

    def down_chunk(c):
        own_weight(2, c).wait()
        other_weight(2, c).wait_recv()

        def one(i):
            j = (i + 1) % n_sp
            parts = [
                dot(arrived[n, j], wd[c, n * step : (n + 1) * step, :]) for n in range(2 * ff // step)
            ]
            value = sum(parts[1:], parts[0]).astype(BF16)

            @pl.when(j > 0)
            def _():
                sent[c, j] = value
                give_back(c, j).start()

            @pl.when(j == 0)
            def _():
                returned[c, j] = value

        loop(n_sp, one)

    loop(chunks, down_chunk)

    def combine_chunk(c):
        shared_weight(2, c).wait()
        for j in range(1, n_sp):
            give_back(c, j).wait_recv()
        held = returned[c].reshape(slots, step)

        def part(i):
            return dot(mix[i], held) + dot(sh[i], sd[c])

        def away(i):
            gathered[c, i] = part(i * 2 + 1 - core).astype(BF16)

        loop(lanes, away)
        cross(c).start()
        cross(c).wait_recv()

        def home(i):
            j = (i + 1) % lanes
            other = (z + j) % lanes
            value = part(other * 2 + core) + x_recv[c, other].astype(F32)
            gathered[c, lanes + j] = value.astype(BF16)

            @pl.when(j > 0)
            def _():
                spread(c, j).start()

        loop(lanes, home)

    loop(chunks, combine_chunk)

    def finish_chunk(c):
        total = gathered[c, lanes].astype(F32)
        for j in range(1, lanes):
            spread(c, j).wait_recv()
        for j in range(1, lanes):
            total += z_recv[c, j].astype(F32)
        out[:, cols(c)] = (after_mix[:, cols(c)].astype(F32) + total).astype(BF16)

    loop(chunks, finish_chunk)

    def settle(c):
        for j in range(1, lanes):
            own_piece(c, j).wait_send()
            spread(c, j).wait_send()
        own_to_partner(c).wait_send()
        for j in range(1, n_sp):
            give_back(c, j).wait_send()
        for n in range(3):
            other_weight(n, c).wait_send()
        cross(c).wait_send()

    loop(chunks, settle)


def moe(normed, after_mix, place_t, place, weight, w_gate, w_up, w_down, s_gate, s_up, s_down):
    n_sp = lax.axis_size("sp")
    n_tp = lax.axis_size("tp")
    lanes = n_tp // 2
    rows, width = normed.shape
    step = width // CHUNKS
    ff = w_gate.shape[1]
    sff = s_gate.shape[0]
    q = rows * n_tp
    half_cap = max(2, 2 * q * TOPK // (n_sp * lanes)) // 2
    slots = n_sp * half_cap
    dma = pltpu.SemaphoreType.DMA
    vm = pltpu.VMEM
    in_vmem = pl.BlockSpec(memory_space=pltpu.VMEM)
    in_hbm = pl.BlockSpec(memory_space=pl.ANY)
    scratch = [
        vm((CHUNKS, 2 * ff, step), BF16),
        vm((CHUNKS, 2 * ff, step), BF16),
        vm((CHUNKS, 2 * ff, step), BF16),
        vm((CHUNKS, 2 * sff, step), BF16),
        vm((CHUNKS, sff, step), BF16),
        vm((CHUNKS, n_tp, rows, step), BF16),
        vm((n_sp, half_cap, q), BF16),
        vm((n_tp, rows, slots), BF16),
        vm((CHUNKS, n_sp, half_cap, step), BF16),
        vm((CHUNKS, n_sp, half_cap, step), BF16),
        vm((2 * ff // TILE, slots, TILE), F32),
        vm((2 * ff // TILE, slots, TILE), F32),
        vm((q, 2 * sff), F32),
        vm((n_tp, rows, sff), BF16),
        vm((CHUNKS, n_sp, half_cap, step), BF16),
        vm((CHUNKS, lanes, rows, step), BF16),
        vm((CHUNKS, lanes, rows, step), BF16),
        dma((3, CHUNKS)),
        dma((3, CHUNKS)),
        dma((3, CHUNKS)),
        dma((3, CHUNKS)),
        dma((CHUNKS, lanes)),
        dma((CHUNKS, lanes)),
        dma((CHUNKS, lanes)),
        dma((CHUNKS, lanes)),
        dma((CHUNKS, n_sp)),
        dma((CHUNKS, n_sp)),
        dma((CHUNKS, n_sp)),
        dma((CHUNKS, n_sp)),
        dma((CHUNKS,)),
        dma((CHUNKS,)),
        dma((CHUNKS, lanes)),
        dma((CHUNKS, lanes)),
    ]
    return pl.pallas_call(
        moe_kernel,
        name="moe",
        out_shape=jax.ShapeDtypeStruct((rows, width), BF16),
        in_specs=[in_vmem] * 5 + [in_hbm] * 6,
        out_specs=in_vmem,
        scratch_shapes=scratch,
        compiler_params=pltpu.CompilerParams(
            collective_id=0, has_side_effects=True, vmem_limit_bytes=67043328
        ),
        cost_estimate=pl.CostEstimate(
            flops=12 * slots * ff * width, bytes_accessed=6 * ff * width, transcendentals=0
        ),
    )(normed, after_mix, place_t, place, weight, w_gate, w_up, w_down, s_gate, s_up, s_down)


def shifted(block, axis, distance):
    devices = range(lax.axis_size(axis))
    route = [(i - distance, i) for i in devices if i - distance in devices]
    return lax.ppermute(block, axis, route)


def normalize(after_mix, norm_gain):
    values_f = after_mix.astype(F32)
    scale = lax.rsqrt(jnp.mean(values_f * values_f, axis=-1, keepdims=True) + 1e-06)
    return (values_f * scale * norm_gain).astype(BF16)


def slot_places(route_ids, route_weights, targets, first_rank):
    named = route_ids[:, :, None] == targets[None, None, :]
    named_f = jnp.sum(named.astype(F32), axis=1)
    weight = jnp.sum(jnp.where(named, route_weights[:, :, None], 0.0), axis=1)
    rows = route_ids.shape[0]
    steps = jnp.arange(rows)
    earlier = (steps[None, :] < steps[:, None]).astype(BF16)
    rank = jnp.dot(earlier, named_f.astype(BF16), preferred_element_type=F32)
    place = jnp.where(named_f > 0, rank - first_rank, -1.0)
    return place, weight


def body(
    queries,
    keys,
    values,
    sink_logits,
    w_out,
    residual,
    norm_gain,
    expert_ids,
    expert_weights,
    w_gate,
    w_up,
    w_down,
    shared_gate,
    shared_up,
    shared_down,
):
    tp_count = lax.axis_size("tp")
    sp_count = lax.axis_size("sp")
    seq_rows = queries.shape[0]
    expert_count = sp_count * tp_count // 2
    capacity = max(2, 2 * seq_rows * TOPK // expert_count)
    local_heads = queries.shape[1] // HD
    kv_start = lax.axis_index("tp") * local_heads // GROUP * HD
    key_cols = lax.dynamic_slice_in_dim(keys, kv_start, HD, 1)
    value_cols = lax.dynamic_slice_in_dim(values, kv_start, HD, 1)
    rim = jnp.concatenate([keys[seq_rows - WINDOW :], values[seq_rows - WINDOW :]], axis=1)
    rim = shifted(rim, "sp", 1)
    rim_keys = lax.dynamic_slice_in_dim(rim, kv_start, HD, 1)
    rim_values = lax.dynamic_slice_in_dim(rim, kv_start + keys.shape[1], HD, 1)
    num_blocks = seq_rows // WINDOW
    key_blocks = key_cols.reshape(num_blocks, WINDOW, HD)
    value_blocks = value_cols.reshape(num_blocks, WINDOW, HD)
    keys_ext = jnp.concatenate(
        [jnp.concatenate([rim_keys[None], key_blocks[:-1]], axis=0), key_blocks], axis=1
    )
    values_ext = jnp.concatenate(
        [jnp.concatenate([rim_values[None], value_blocks[:-1]], axis=0), value_blocks], axis=1
    )
    query_blocks = queries.reshape(num_blocks, WINDOW, local_heads, HD)
    scores = jnp.einsum(
        "nqhd,nsd->nhqs", query_blocks, keys_ext, preferred_element_type=F32
    ) * HD ** (-0.5)
    query_pos = jnp.arange(WINDOW)[:, None] + WINDOW
    key_pos = jnp.arange(2 * WINDOW)[None, :]
    in_band = (key_pos <= query_pos) & (key_pos > query_pos - WINDOW)
    absolute = (
        lax.axis_index("sp") * seq_rows
        + jnp.arange(num_blocks)[:, None, None] * WINDOW
        + key_pos[None]
        - WINDOW
    )
    allowed = in_band[None] & (absolute >= 0)
    scores = jnp.where(allowed[:, None], scores, -jnp.inf)
    sink_col = jnp.broadcast_to(sink_logits[None, :, None, None], scores.shape[:-1] + (1,))
    combined = jnp.concatenate([scores, sink_col], axis=-1)
    row_max = jnp.max(combined, axis=-1, keepdims=True)
    exps = jnp.exp(combined - row_max)
    weights = (exps[..., :-1] / jnp.sum(exps, axis=-1, keepdims=True)).astype(BF16)
    attended = jnp.einsum("nhqs,nsd->nqhd", weights, values_ext, preferred_element_type=F32)
    attended = attended.astype(BF16).reshape(seq_rows, local_heads * HD)
    head_rows = lax.all_to_all(attended, "tp", split_axis=0, concat_axis=1, tiled=True)
    projected = jnp.dot(
        head_rows,
        lax.all_gather(w_out, "tp", axis=0, tiled=True),
        preferred_element_type=F32,
    )
    after_mix = (residual.astype(F32) + projected).astype(BF16)
    normed = normalize(after_mix, norm_gain)
    tp_index = lax.axis_index("tp")
    sp_index = lax.axis_index("sp")
    lanes = tp_count // 2
    lane = tp_index // 2
    half_cap = capacity // 2
    columns = (jnp.arange(sp_count, dtype=jnp.int32) + sp_index) % sp_count
    targets = columns * lanes + lane
    first_rank = (tp_index % 2 * half_cap).astype(F32)
    place, weight = slot_places(expert_ids, expert_weights, targets, first_rank)
    rows = after_mix.shape[0]
    return moe(
        normed,
        after_mix,
        place.T.reshape(sp_count, 1, seq_rows),
        place.reshape(tp_count, rows, sp_count),
        weight.reshape(tp_count, rows, sp_count),
        w_gate,
        w_up,
        w_down,
        shared_gate,
        shared_up,
        shared_down,
    )


def solution(mesh):
    return jax.shard_map(
        body,
        mesh=mesh,
        in_specs=(
            P("sp", "tp"),
            P("sp", None),
            P("sp", None),
            P("tp"),
            P("tp", None),
            P(("sp", "tp"), None),
            P(),
            P("sp", None),
            P("sp", None),
            P(("sp", "tp"), None, None),
            P(("sp", "tp"), None, None),
            P(("sp", "tp"), None, None),
            P("tp", None),
            P("tp", None),
            P("tp", None),
        ),
        out_specs=P(("sp", "tp"), None),
        check_vma=False,
    )
```

time: 310 us -> 229 us (0.74)
  Pallas kernels: 0 us -> 152 us
  waiting for transfers between devices: 135 us -> 33.8 us
  matrix products: 77.5 us -> 5.09 us
  blocking collectives: 47 us -> 0 us
  starting transfers between devices: 17.9 us -> 8.91 us
  other arithmetic: 6.92 us -> 1.98 us
  local copies, waits for them, and re-layouts: 7.28 us -> 10.7 us
    pallas_call x0 -> x1, Pallas kernels: none -> 152 us  [moe(): pl.pallas_call(moe_kernel, name='moe', out_shape=jax.ShapeDtypeStruct((ro...]
    dot_general x24 -> x1, matrix products: 73.6 us -> 0.46 us  [slot_places(): rank = jnp.dot(earlier, named_f.astype(BF16), preferred_element_type=F32)]
    all_to_all x2 -> x0, blocking collectives: 47 us -> none  [the longest x1 26.4 us: body(): lax.all_to_all(outs[c], 'sp', split_axis=0, concat_axis=0, tiled=True)]
    all_gather x2 -> x0, waiting for transfers between devices: 45.6 us -> none  [body(): rows = lax.all_gather(normed[:, cols], 'tp', axis=0, tiled=True)]
    reduce_scatter x2 -> x0, waiting for transfers between devices: 41.7 us -> none  [body(): lax.psum_scatter(part.astype(jnp.bfloat16), 'tp', scatter_dimension=0, ti...]
    all_to_all x3 -> x1, waiting for transfers between devices: 24.1 us -> 11.9 us  [body(): lax.all_to_all(attended, 'tp', split_axis=0, concat_axis=1, tiled=True)]
    all_to_all x3 -> x1, starting transfers between devices: 13.4 us -> 5.79 us  [body(): lax.all_to_all(attended, 'tp', split_axis=0, concat_axis=1, tiled=True)]
    convert_element_type x6 -> x1, other arithmetic: 5.81 us -> 0.98 us  [normalize(): return (values_f * scale * norm_gain).astype(BF16)]
  transfers between devices with their start and end apart: 12 -> 3, of which waited for: 8 -> 2; matrix products, arithmetic and copies ran while one was open for 16% -> 5% of each run, Pallas kernels for 0% -> 0%
where the time goes in v1:
time: 229 us; the launch traced here: 226 us
  Pallas kernels  152 us (66%)
  waiting for transfers between devices  33.8 us (15%)
  between operations  13.6 us (6%)
  local copies, waits for them, and re-layouts  10.7 us (5%)
  starting transfers between devices  8.91 us (4%)
  matrix products  5.09 us (2%)
    pallas_call x1, Pallas kernels, moe(): pl.pallas_call(moe_kernel, name='moe', out_shape=jax.ShapeDtypeStruct((ro...  152 us
    all_gather x1, waiting for transfers between devices, body(): lax.all_gather(w_out, 'tp', axis=0, tiled=True)  21.2 us
    all_to_all x1, waiting for transfers between devices, body(): lax.all_to_all(attended, 'tp', split_axis=0, concat_axis=1, tiled=True)  11.9 us
    all_to_all x1, starting transfers between devices, body(): lax.all_to_all(attended, 'tp', split_axis=0, concat_axis=1, tiled=True)  5.79 us
  transfers between devices with their start and end apart: 3, of which 2 were waited for; matrix products, arithmetic and copies ran while one was open for 5% of the time, Pallas kernels for 0%

profile of v1, /device:TPU:27, one launch (start us, length us, event | category | flops | bytes accessed | tf_op | source)
XLA Modules:
  0.0 226.2 jit_solution(8880263773277201224)
XLA Ops:
  6.5 0.0 copy-start.2
  6.5 0.0 all-gather.2.cloned.1.call-start
  6.5 0.7 all-gather.2.cloned.1.call-update
  7.3 0.8 slice.21
  8.1 0.8 slice.22
  9.0 3.1 %collective-permute-start = (bf16[128,512]{1,0:T(8,128)(2,1)S(1)}, bf16[128,512]{1,0:T(8,128)(2,1)S(1)}, u32[]{:S(2)}, u32[]{:S(2)}) collective-permute-start(bf16[128,512]{1,0:T(8,128)(2,1)S(1)} %pad_maximum_fusion), channel_id=1, source_target_pairs={{0,8},{8,16},{16,24},{1,9},{9,17},{17,25},{2,10},{10,18},{18,26},{... | collective-permute-start | bytes 393224 | tf_op jit(solution)/shard_map/ppermute | solution.py:452
  12.1 1.2 constant_dynamic-slice_fusion.2
  13.4 0.1 copy.48
  13.5 1.2 constant_dynamic-slice_fusion
  14.8 0.1 copy.46
  14.9 0.0 copy-done.2
  14.9 0.2 reshape.153
  15.2 0.1 copy.43
  15.3 0.1 copy.41
  15.5 0.0 copy-start.6
  15.5 0.1 add_compare_fusion
  15.6 0.3 broadcast_and_fusion
  16.0 0.0 collective-permute-done
  16.0 0.1 constant_dynamic-slice_fusion.5
  16.1 0.1 copy.44
  16.2 0.1 copy.39
  16.3 0.6 fusion.29
  16.8 0.0 copy-done.6
  16.8 0.1 broadcast_maximum_fusion
  16.9 0.1 broadcast_in_dim.60
  17.0 0.3 fusion.28
  17.3 0.0 copy-start.3
  17.3 0.0 copy-start.4
  17.3 1.0 convolution_convert_fusion
  18.4 0.0 copy-start.1
  18.4 5.8 %all-to-all-start = ((bf16[8,128,128]{1,2,0:T(8,128)(2,1)}), bf16[8,128,128]{1,2,0:T(8,128)(2,1)S(1)}, u32[]{:S(2)}, u32[]{:S(2)}) async-start(bf16[8,128,128]{1,2,0:T(8,128)(2,1)} %bitcast.12), calls=%async_computation | async-start | bytes 524288 | tf_op jit(solution)/shard_map/all_to_all | solution.py:534
  24.2 0.0 copy-done.3
  24.2 0.0 copy-done.4
  24.2 0.1 fusion.21
  24.3 0.5 fusion.5
  24.8 1.1 copy.52
  25.8 1.0 copy.53
  26.9 0.6 reshape.148.place_t
  27.5 11.9 %all-to-all-done = bf16[8,128,128]{1,2,0:T(8,128)(2,1)S(1)} async-done(((bf16[8,128,128]{1,2,0:T(8,128)(2,1)}), bf16[8,128,128]{1,2,0:T(8,128)(2,1)S(1)}, u32[]{:S(2)}, u32[]{:S(2)}) %all-to-all-start) | async-done | bytes 262176 | tf_op jit(solution)/shard_map/all_to_all | solution.py:534
  39.4 21.2 %all-gather.2.cloned.1.call-done = bf16[1024,2048]{1,0:T(8,128)(2,1)} async-done(((bf16[128,2048]{1,0:T(8,128)(2,1)}), bf16[1024,2048]{1,0:T(8,128)(2,1)}) %all-gather.2.cloned.1.call-update) | async-done | bytes 4194320 | tf_op jit(solution)/shard_map/all_gather | solution.py:537
  60.6 0.0 copy-done.1
  60.6 3.0 %fusion.6 = (f32[128]{0:T(128)S(1)}, bf16[128,2048]{1,0:T(8,128)(2,1)S(1)}) fusion(bf16[128,1024]{0,1:T(8,128)(2,1)S(1)} %bitcast.31, bf16[1024,2048]{1,0:T(8,128)(2,1)} %all-gather.2.cloned.1.call-done, bf16[128,2048]{1,0:T(8,128)(2,1)S(1)} %copy-done.1), kind=kOutput, calls=%fused_computation.14 | convolution fusion | flops 538443648 | bytes 5505536 | tf_op jit(solution)/shard_map/dot_general | solution.py:535
  63.6 0.0 copy-start
  63.6 0.8 copy-done
  64.4 0.0 copy-done.5
  64.4 1.0 fusion.8.normed
  65.4 152.1 %moe.1 = bf16[128,2048]{1,0:T(8,128)(2,1)} custom-call(bf16[128,2048]{1,0:T(8,128)(2,1)} %fusion.8.normed, bf16[128,2048]{1,0:T(8,128)(2,1)} %copy-done, f32[4,1,1024]{2,1,0:T(1,128)} %reshape.148.place_t, f32[8,128,4]{2,1,0:T(8,128)} %bitcast.36, f32[8,128,4]{2,1,0:T(8,128)} %bitcast.37, bf16[1,768,2048]{2,1,0:T(8,128)(2,1)} %w_gate.1, ...), custom_call_target="tpu_custom_call" | custom-call | flops 19327352832 | bytes 9437184 | tf_op jit(solution)/shard_map/moe/pallas_call | solution.py:433
  217.5 1.9 copy.72
  (7 shorter events, 0.1 us)
Async XLA Ops:
  6.5 8.4 %copy-start.2 = (bf16[1024,128]{1,0:T(8,128)(2,1)S(1)}, bf16[1024,128]{1,0:T(8,128)(2,1)}, u32[]{:S(2)}) copy-start(bf16[1024,128]{1,0:T(8,128)(2,1)} %param.15) | copy-start | bytes 786436
  6.5 54.0 %all-gather.2.cloned.1.call-start = ((), (), s32[]{:S(2)}) async-start(), calls=%async_computation.1 | async-start | bytes 4718592 | tf_op jit(solution)/shard_map/all_gather | solution.py:537
  9.0 7.0 %collective-permute-start = (bf16[128,512]{1,0:T(8,128)(2,1)S(1)}, bf16[128,512]{1,0:T(8,128)(2,1)S(1)}, u32[]{:S(2)}, u32[]{:S(2)}) collective-permute-start(bf16[128,512]{1,0:T(8,128)(2,1)S(1)} %pad_maximum_fusion), channel_id=1, source_target_pairs={{0,8},{8,16},{16,24},{1,9},{9,17},{17,25},{2,10},{10,18},{18,26},{... | collective-permute-start | bytes 393224 | tf_op jit(solution)/shard_map/ppermute | solution.py:452
  15.5 1.4 copy-start.6
  17.3 6.9 %copy-start.3 = (f32[1024,4]{0,1:T(4,128)S(1)}, f32[1024,4]{0,1:T(4,128)}, u32[]{:S(2)}) copy-start(f32[1024,4]{0,1:T(4,128)} %param.23) | copy-start | bytes 49156
  17.3 6.9 %copy-start.4 = (s32[1024,4]{0,1:T(4,128)S(1)}, s32[1024,4]{0,1:T(4,128)}, u32[]{:S(2)}) copy-start(s32[1024,4]{0,1:T(4,128)} %param.22) | copy-start | bytes 49156
  18.4 42.2 %copy-start.1 = (bf16[128,2048]{1,0:T(8,128)(2,1)S(1)}, bf16[128,2048]{1,0:T(8,128)(2,1)}, u32[]{:S(2)}) copy-start(bf16[128,2048]{1,0:T(8,128)(2,1)} %param.20) | copy-start | bytes 1572868
  18.4 21.0 %all-to-all-start = ((bf16[8,128,128]{1,2,0:T(8,128)(2,1)}), bf16[8,128,128]{1,2,0:T(8,128)(2,1)S(1)}, u32[]{:S(2)}, u32[]{:S(2)}) async-start(bf16[8,128,128]{1,2,0:T(8,128)(2,1)} %bitcast.12), calls=%async_computation | async-start | bytes 524288 | tf_op jit(solution)/shard_map/all_to_all | solution.py:534
  60.6 3.8 %copy-start.5 = (f32[2048]{0:T(1024)S(1)}, f32[2048]{0:T(1024)}, u32[]{:S(2)}) copy-start(f32[2048]{0:T(1024)} %param.21) | copy-start | bytes 24580
  63.6 0.8 copy-start
Sparse Core Ops, SparseCore 0:
  8.9 51.6 all-gather.1

commit v2 on v1

--- a/solution.py
+++ b/solution.py
@@ -35,12 +35,15 @@
     lax.fori_loop(0, n, lambda i, carry: (body(i), carry)[1], 0)
 
 
-def moe_kernel(
-    normed,
-    after_mix,
-    place_t,
-    place,
-    weight,
+def layer_kernel(
+    queries,
+    sinks,
+    info,
+    gain,
+    keys,
+    values,
+    w_out,
+    residual,
     w_gate,
     w_up,
     w_down,
@@ -81,6 +84,25 @@
     x_rsem,
     z_ssem,
     z_rsem,
+    k_ext,
+    v_ext,
+    attended,
+    heads,
+    after_mix,
+    place_t,
+    place,
+    weight,
+    l_sem,
+    rim_send,
+    rim_recv,
+    wz_send,
+    wz_recv,
+    wx_send,
+    wx_recv,
+    h_send,
+    h_recv,
+    p_send,
+    p_recv,
 ):
     n_sp = lax.axis_size("sp")
     n_tp = lax.axis_size("tp")
@@ -89,7 +111,10 @@
     t = lax.axis_index("tp")
     z = t // 2
     core = t % 2
-    rows = normed.shape[0]
+    rows = after_mix.shape[0]
+    width = after_mix.shape[1]
+    head_cols = w_out.shape[0]
+    seq_rows = n_tp * rows
     chunks, _, _, step = gathered.shape
     half_cap = sent.shape[2]
     slots = n_sp * half_cap
@@ -123,10 +148,10 @@
         )
 
     def own_piece(c, j):
-        return remote(normed.at[:, cols(c)], gathered.at[c, t], ag_send.at[c, j], ag_recv.at[c, j], z_peer(j))
+        return remote(gathered.at[c, t], gathered.at[c, t], ag_send.at[c, j], ag_recv.at[c, j], z_peer(j))
 
     def own_to_partner(c):
-        return remote(normed.at[:, cols(c)], gathered.at[c, t], fw_send.at[c, 0], fw_recv.at[c, 0], partner)
+        return remote(gathered.at[c, t], gathered.at[c, t], fw_send.at[c, 0], fw_recv.at[c, 0], partner)
 
     def forward(c, j):
         src = gathered.at[c, ((z + lanes - j) % lanes) * 2 + core]
@@ -165,32 +190,145 @@
         src, dst = shared[n]
         return pltpu.make_async_copy(src.at[:, cols(c)], dst(c), s_sem.at[n, c])
 
-    def start_sends(c):
-        for j in range(1, lanes):
-            own_piece(c, j).start()
-        own_to_partner(c).start()
-
-    loop(chunks, start_sends)
+    group_width = min(width // n_sp, step)
+    groups = width // group_width // n_sp
+
+    def group_at(sp, g, lane):
+        first = (sp * groups + g) * group_width
+        band = pl.ds(pl.multiple_of(first % step, group_width), group_width)
+        return wd.at[first // step, pl.ds(pl.multiple_of(lane * head_cols, head_cols), head_cols), band]
+
+    def group_of_mine(g):
+        first = (s * groups + g) * group_width
+        return w_out.at[:, pl.ds(pl.multiple_of(first, group_width), group_width)]
+
+    def out_shard(g, j):
+        return remote(group_of_mine(g), group_at(s, g, z), wz_send.at[g, j], wz_recv.at[g, j], z_peer(j))
+
+    def out_relay(g, j, i):
+        block = group_at(s, g, (z + lanes - j) % lanes)
+        return remote(block, block, wx_send.at[g, j, i], wx_recv.at[g, j, i], sp_peer(i))
+
+    def out_own(c):
+        mine = wd.at[c, pl.ds(pl.multiple_of(z * head_cols, head_cols), head_cols)]
+        return pltpu.make_async_copy(w_out.at[:, cols(c)], mine, l_sem.at[3, c])
+
+    kv_start = t * head_cols // HD // GROUP * HD
+    kv_cols = pl.ds(pl.multiple_of(kv_start // 128 * 128, 128), 128)
+    parity = kv_start // HD % 2
+
+    def rim(src, dst, n):
+        last = src.at[pl.ds(seq_rows - WINDOW, WINDOW), kv_cols]
+        return remote(last, dst.at[0:WINDOW], rim_send.at[n], rim_recv.at[n], sp_peer(1))
+
+    def own_kv(src, dst, n):
+        return pltpu.make_async_copy(src.at[:, kv_cols], dst.at[WINDOW : WINDOW + seq_rows], l_sem.at[n, 0])
+
+    own_residual = pltpu.make_async_copy(residual, after_mix, l_sem.at[2, 0])
+    rim(keys, k_ext, 0).start()
+    rim(values, v_ext, 1).start()
+    own_kv(keys, k_ext, 0).start()
+    own_kv(values, v_ext, 1).start()
+    for g in range(groups):
+        for j in range(1, lanes):
+            out_shard(g, j).start()
+    own_residual.start()
 
     def start_weights(c):
+        out_own(c).start()
         for n in range(2):
             own_weight(n, c).start()
             other_weight(n, c).start()
             shared_weight(n, c).start()
-
-    loop(chunks, start_weights)
-
-    def start_down(c):
-        own_weight(2, c).start()
         other_weight(2, c).start()
         shared_weight(2, c).start()
 
-    loop(chunks, start_down)
-
-    def keep_own(c):
-        gathered[c, t] = normed[:, cols(c)]
-
-    loop(chunks, keep_own)
+    own_kv(keys, k_ext, 0).wait()
+    own_kv(values, v_ext, 1).wait()
+    loop(chunks, start_weights)
+    rim(keys, k_ext, 0).wait_recv()
+    rim(values, v_ext, 1).wait_recv()
+
+    lane_id = lax.broadcasted_iota(jnp.int32, (1, 128), 1)
+    query_row = lax.broadcasted_iota(jnp.int32, (2 * rows, 1), 0)
+    in_block = query_row % rows
+    key_at = lax.broadcasted_iota(jnp.int32, (1, rows + WINDOW), 1)
+    band_mask = (key_at <= in_block + WINDOW) & (key_at > in_block)
+    sink = jnp.where(query_row < rows, sinks[0], sinks[1])
+
+    def attend(block):
+        first = pl.multiple_of(block * rows, rows)
+        q = queries[pl.ds(first, rows), :].astype(F32) * HD ** (-0.5)
+        turned = pltpu.roll(q, 64, 1)
+        mine = lane_id // HD == parity
+        q0 = jnp.where(mine, jnp.where(parity == 0, q, turned), 0.0)
+        q1 = jnp.where(mine, jnp.where(parity == 1, q, turned), 0.0)
+        q2 = jnp.concatenate([q0, q1], axis=0).astype(BF16)
+        scores = dot_t(q2, k_ext[pl.ds(first, rows + WINDOW), :])
+        allowed = band_mask & (s * seq_rows + first + key_at >= WINDOW)
+        scores = jnp.where(allowed, scores, -1e30)
+        top = jnp.maximum(jnp.max(scores, axis=1, keepdims=True), sink)
+        exps = jnp.exp(scores - top)
+        total = jnp.sum(exps, axis=1, keepdims=True) + jnp.exp(sink - top)
+        probs = (exps / total).astype(BF16)
+        o = dot(probs, v_ext[pl.ds(first, rows + WINDOW), :])
+        o0, o1 = o[0:rows], o[rows : 2 * rows]
+        o0 = jnp.where(parity == 0, o0, pltpu.roll(o0, 64, 1))
+        o1 = jnp.where(parity == 1, o1, pltpu.roll(o1, 64, 1))
+        return jnp.where(lane_id < HD, o0, o1).astype(BF16)
+
+    def head_rows(j):
+        return remote(attended.at[j], heads.at[z], h_send.at[j], h_recv.at[j], z_peer(j))
+
+    def attend_chip(i):
+        j = (i + 1) % lanes
+        other = (z + j) % lanes
+
+        def half(n):
+            value = attend(other * 2 + n)
+
+            @pl.when(j > 0)
+            def _():
+                attended[j, pl.ds(pl.multiple_of(n * rows, rows), rows), :] = value
+
+            @pl.when(j == 0)
+            def _():
+                heads[z, pl.ds(pl.multiple_of(n * rows, rows), rows), :] = value
+
+        loop(2, half)
+
+        @pl.when(j > 0)
+        def _():
+            head_rows(j).start()
+
+    loop(lanes, attend_chip)
+
+    for g in range(groups):
+        for j in range(1, lanes):
+            out_shard(g, j).wait_recv()
+            for i in range(1, n_sp):
+                out_relay(g, j, i).start()
+
+    lane_q = lax.broadcasted_iota(jnp.int32, (1, seq_rows), 1)
+    named_rows, weight_rows = [], []
+    for j in range(n_sp):
+        target = ((s + j) % n_sp * lanes + z).astype(F32)
+        hit = info[0:TOPK] == target
+        named_rows.append(jnp.max(jnp.where(hit, 1.0, 0.0), axis=0, keepdims=True))
+        weight_rows.append(jnp.sum(jnp.where(hit, info[TOPK : 2 * TOPK], 0.0), axis=0, keepdims=True))
+    fill = [jnp.zeros((1, seq_rows), F32)] * (-n_sp % 8)
+    named = jnp.concatenate(named_rows + fill, axis=0)
+    scan = named
+    apart = 1
+    while apart < seq_rows:
+        scan = scan + jnp.where(lane_q >= apart, pltpu.roll(scan, apart, 1), 0.0)
+        apart *= 2
+    half_at = (core * half_cap).astype(F32)
+    places = jnp.where(named > 0, scan - named - half_at, -1.0)
+    for j in range(n_sp):
+        place_t[j] = places[j : j + 1]
+    place[...] = places.T.reshape(place.shape)
+    weight[...] = jnp.concatenate(weight_rows + fill, axis=0).T.reshape(weight.shape)
 
     slot_down = lax.broadcasted_iota(jnp.int32, (half_cap, 1), 0).astype(F32)
     slot_along = lax.broadcasted_iota(jnp.int32, (1, half_cap), 1).astype(F32)
@@ -209,6 +347,63 @@
 
     loop(n_tp, build_mix)
 
+    for j in range(1, lanes):
+        head_rows(j).wait_recv()
+    for g in range(groups):
+        for j in range(1, lanes):
+            for i in range(1, n_sp):
+                out_relay(g, j, i).wait_recv()
+    for c in range(chunks):
+        out_own(c).wait()
+    own_residual.wait()
+
+    def stripe(c):
+        return pl.ds(pl.multiple_of(c * per * rows, per * rows), per * rows)
+
+    def exchange(c):
+        return remote(
+            acc_g.at[1 - core, stripe(c)], acc_g.at[2, stripe(c)], p_send.at[c], p_recv.at[c], partner
+        )
+
+    def project(c):
+        parts = [
+            dot(heads[i][:, 0:head_cols], wd[c, i * head_cols : (i + 1) * head_cols, :]) for i in range(lanes)
+        ]
+        value = sum(parts[1:], parts[0])
+        for n in range(2):
+            for p in range(per):
+                at = pl.ds(pl.multiple_of((c * per + p) * rows, rows), rows)
+                acc_g[n, at, :] = value[n * rows : (n + 1) * rows, p * TILE : (p + 1) * TILE]
+        exchange(c).start()
+
+    loop(chunks, project)
+    for g in range(groups):
+        for j in range(1, lanes):
+            for i in range(1, n_sp):
+                out_relay(g, j, i).wait_send()
+    for c in range(chunks):
+        own_weight(2, c).start()
+    squares = jnp.zeros((rows, 1), F32)
+    for c in range(chunks):
+        exchange(c).wait_recv()
+        for p in range(per):
+            k = c * per + p
+            at = pl.ds(k * rows, rows)
+            band = slice(k * TILE, (k + 1) * TILE)
+            value = after_mix[:, band].astype(F32) + (acc_g[core, at, :] + acc_g[2, at, :])
+            value = value.astype(BF16)
+            after_mix[:, band] = value
+            squares += jnp.sum(value.astype(F32) * value.astype(F32), axis=1, keepdims=True)
+    scale = lax.rsqrt(squares / width + 1e-06)
+    for c in range(chunks):
+        band = slice(c * step, (c + 1) * step)
+        gathered[c, t] = (after_mix[:, band].astype(F32) * scale * gain[:, band]).astype(BF16)
+        for j in range(1, lanes):
+            own_piece(c, j).start()
+        own_to_partner(c).start()
+    for c in range(chunks):
+        exchange(c).wait_send()
+
     def gather_chunk(c):
         for j in range(1, lanes):
             own_piece(c, j).wait_recv()
@@ -298,7 +493,9 @@
         for j in range(1, n_sp):
             dispatch(c, j).wait_send()
         for j in range(1, lanes):
+            own_piece(c, j).wait_send()
             forward(c, j).wait_send()
+        own_to_partner(c).wait_send()
 
     loop(chunks, settle_dispatch)
 
@@ -368,9 +565,7 @@
 
     def settle(c):
         for j in range(1, lanes):
-            own_piece(c, j).wait_send()
             spread(c, j).wait_send()
-        own_to_partner(c).wait_send()
         for j in range(1, n_sp):
             give_back(c, j).wait_send()
         for n in range(3):
@@ -378,22 +573,33 @@
         cross(c).wait_send()
 
     loop(chunks, settle)
-
-
-def moe(normed, after_mix, place_t, place, weight, w_gate, w_up, w_down, s_gate, s_up, s_down):
+    rim(keys, k_ext, 0).wait_send()
+    rim(values, v_ext, 1).wait_send()
+    for j in range(1, lanes):
+        head_rows(j).wait_send()
+        for g in range(groups):
+            out_shard(g, j).wait_send()
+
+
+def layer(
+    queries, sinks, info, gain, keys, values, w_out, residual, w_gate, w_up, w_down, s_gate, s_up, s_down
+):
     n_sp = lax.axis_size("sp")
     n_tp = lax.axis_size("tp")
     lanes = n_tp // 2
-    rows, width = normed.shape
+    rows, width = residual.shape
     step = width // CHUNKS
     ff = w_gate.shape[1]
     sff = s_gate.shape[0]
     q = rows * n_tp
     half_cap = max(2, 2 * q * TOPK // (n_sp * lanes)) // 2
     slots = n_sp * half_cap
+    groups = width // min(width // n_sp, step) // n_sp
+    padded = -(-n_sp // 8) * 8
     dma = pltpu.SemaphoreType.DMA
     vm = pltpu.VMEM
     in_vmem = pl.BlockSpec(memory_space=pltpu.VMEM)
+    in_smem = pl.BlockSpec(memory_space=pltpu.SMEM)
     in_hbm = pl.BlockSpec(memory_space=pl.ANY)
     scratch = [
         vm((CHUNKS, 2 * ff, step), BF16),
@@ -429,12 +635,31 @@
         dma((CHUNKS,)),
         dma((CHUNKS, lanes)),
         dma((CHUNKS, lanes)),
+        vm((q + WINDOW, 128), BF16),
+        vm((q + WINDOW, 128), BF16),
+        vm((lanes, 2 * rows, 128), BF16),
+        vm((lanes, 2 * rows, 128), BF16),
+        vm((rows, width), BF16),
+        vm((n_sp, 1, q), F32),
+        vm((n_tp, rows, padded), F32),
+        vm((n_tp, rows, padded), F32),
+        dma((4, CHUNKS)),
+        dma((2,)),
+        dma((2,)),
+        dma((groups, lanes)),
+        dma((groups, lanes)),
+        dma((groups, lanes, n_sp)),
+        dma((groups, lanes, n_sp)),
+        dma((lanes,)),
+        dma((lanes,)),
+        dma((CHUNKS,)),
+        dma((CHUNKS,)),
     ]
     return pl.pallas_call(
-        moe_kernel,
-        name="moe",
+        layer_kernel,
+        name="layer",
         out_shape=jax.ShapeDtypeStruct((rows, width), BF16),
-        in_specs=[in_vmem] * 5 + [in_hbm] * 6,
+        in_specs=[in_vmem, in_smem, in_vmem, in_vmem] + [in_hbm] * 10,
         out_specs=in_vmem,
         scratch_shapes=scratch,
         compiler_params=pltpu.CompilerParams(
@@ -443,31 +668,7 @@
         cost_estimate=pl.CostEstimate(
             flops=12 * slots * ff * width, bytes_accessed=6 * ff * width, transcendentals=0
         ),
-    )(normed, after_mix, place_t, place, weight, w_gate, w_up, w_down, s_gate, s_up, s_down)
-
-
-def shifted(block, axis, distance):
-    devices = range(lax.axis_size(axis))
-    route = [(i - distance, i) for i in devices if i - distance in devices]
-    return lax.ppermute(block, axis, route)
-
-
-def normalize(after_mix, norm_gain):
-    values_f = after_mix.astype(F32)
-    scale = lax.rsqrt(jnp.mean(values_f * values_f, axis=-1, keepdims=True) + 1e-06)
-    return (values_f * scale * norm_gain).astype(BF16)
-
-
-def slot_places(route_ids, route_weights, targets, first_rank):
-    named = route_ids[:, :, None] == targets[None, None, :]
-    named_f = jnp.sum(named.astype(F32), axis=1)
-    weight = jnp.sum(jnp.where(named, route_weights[:, :, None], 0.0), axis=1)
-    rows = route_ids.shape[0]
-    steps = jnp.arange(rows)
-    earlier = (steps[None, :] < steps[:, None]).astype(BF16)
-    rank = jnp.dot(earlier, named_f.astype(BF16), preferred_element_type=F32)
-    place = jnp.where(named_f > 0, rank - first_rank, -1.0)
-    return place, weight
+    )(queries, sinks, info, gain, keys, values, w_out, residual, w_gate, w_up, w_down, s_gate, s_up, s_down)
 
 
 def body(
@@ -487,74 +688,20 @@
     shared_up,
     shared_down,
 ):
-    tp_count = lax.axis_size("tp")
-    sp_count = lax.axis_size("sp")
-    seq_rows = queries.shape[0]
-    expert_count = sp_count * tp_count // 2
-    capacity = max(2, 2 * seq_rows * TOPK // expert_count)
-    local_heads = queries.shape[1] // HD
-    kv_start = lax.axis_index("tp") * local_heads // GROUP * HD
-    key_cols = lax.dynamic_slice_in_dim(keys, kv_start, HD, 1)
-    value_cols = lax.dynamic_slice_in_dim(values, kv_start, HD, 1)
-    rim = jnp.concatenate([keys[seq_rows - WINDOW :], values[seq_rows - WINDOW :]], axis=1)
-    rim = shifted(rim, "sp", 1)
-    rim_keys = lax.dynamic_slice_in_dim(rim, kv_start, HD, 1)
-    rim_values = lax.dynamic_slice_in_dim(rim, kv_start + keys.shape[1], HD, 1)
-    num_blocks = seq_rows // WINDOW
-    key_blocks = key_cols.reshape(num_blocks, WINDOW, HD)
-    value_blocks = value_cols.reshape(num_blocks, WINDOW, HD)
-    keys_ext = jnp.concatenate(
-        [jnp.concatenate([rim_keys[None], key_blocks[:-1]], axis=0), key_blocks], axis=1
-    )
-    values_ext = jnp.concatenate(
-        [jnp.concatenate([rim_values[None], value_blocks[:-1]], axis=0), value_blocks], axis=1
-    )
-    query_blocks = queries.reshape(num_blocks, WINDOW, local_heads, HD)
-    scores = jnp.einsum(
-        "nqhd,nsd->nhqs", query_blocks, keys_ext, preferred_element_type=F32
-    ) * HD ** (-0.5)
-    query_pos = jnp.arange(WINDOW)[:, None] + WINDOW
-    key_pos = jnp.arange(2 * WINDOW)[None, :]
-    in_band = (key_pos <= query_pos) & (key_pos > query_pos - WINDOW)
-    absolute = (
-        lax.axis_index("sp") * seq_rows
-        + jnp.arange(num_blocks)[:, None, None] * WINDOW
-        + key_pos[None]
-        - WINDOW
-    )
-    allowed = in_band[None] & (absolute >= 0)
-    scores = jnp.where(allowed[:, None], scores, -jnp.inf)
-    sink_col = jnp.broadcast_to(sink_logits[None, :, None, None], scores.shape[:-1] + (1,))
-    combined = jnp.concatenate([scores, sink_col], axis=-1)
-    row_max = jnp.max(combined, axis=-1, keepdims=True)
-    exps = jnp.exp(combined - row_max)
-    weights = (exps[..., :-1] / jnp.sum(exps, axis=-1, keepdims=True)).astype(BF16)
-    attended = jnp.einsum("nhqs,nsd->nqhd", weights, values_ext, preferred_element_type=F32)
-    attended = attended.astype(BF16).reshape(seq_rows, local_heads * HD)
-    head_rows = lax.all_to_all(attended, "tp", split_axis=0, concat_axis=1, tiled=True)
-    projected = jnp.dot(
-        head_rows,
-        lax.all_gather(w_out, "tp", axis=0, tiled=True),
-        preferred_element_type=F32,
-    )
-    after_mix = (residual.astype(F32) + projected).astype(BF16)
-    normed = normalize(after_mix, norm_gain)
-    tp_index = lax.axis_index("tp")
-    sp_index = lax.axis_index("sp")
-    lanes = tp_count // 2
-    lane = tp_index // 2
-    half_cap = capacity // 2
-    columns = (jnp.arange(sp_count, dtype=jnp.int32) + sp_index) % sp_count
-    targets = columns * lanes + lane
-    first_rank = (tp_index % 2 * half_cap).astype(F32)
-    place, weight = slot_places(expert_ids, expert_weights, targets, first_rank)
-    rows = after_mix.shape[0]
-    return moe(
-        normed,
-        after_mix,
-        place.T.reshape(sp_count, 1, seq_rows),
-        place.reshape(tp_count, rows, sp_count),
-        weight.reshape(tp_count, rows, sp_count),
+    spare = 128 - queries.shape[1]
+    if spare > 0:
+        queries = jnp.pad(queries, ((0, 0), (0, spare)))
+        sink_logits = jnp.pad(sink_logits, (0, spare // HD))
+    info = jnp.concatenate([expert_ids.T.astype(F32), expert_weights.T], axis=0)
+    return layer(
+        queries,
+        sink_logits,
+        info,
+        norm_gain[None],
+        keys,
+        values,
+        w_out,
+        residual,
         w_gate,
         w_up,
         w_down,

time: 229 us -> 186 us (0.81)
  waiting for transfers between devices: 33.8 us -> 0 us
  Pallas kernels: 152 us -> 181 us
  between operations: 13.6 us -> 0.01 us
  starting transfers between devices: 8.91 us -> 0 us
  local copies, waits for them, and re-layouts: 10.7 us -> 1.88 us
  matrix products: 5.09 us -> 0 us
    pallas_call x1, Pallas kernels: 152 us -> 181 us  [layer(): pl.pallas_call(layer_kernel, name='layer', out_shape=jax.ShapeDtypeStruct...]
    all_gather x1 -> x0, waiting for transfers between devices: 21.2 us -> none  [body(): lax.all_gather(w_out, 'tp', axis=0, tiled=True)]
    all_to_all x1 -> x0, waiting for transfers between devices: 11.9 us -> none  [body(): lax.all_to_all(attended, 'tp', split_axis=0, concat_axis=1, tiled=True)]
    all_to_all x1 -> x0, starting transfers between devices: 5.79 us -> none  [body(): lax.all_to_all(attended, 'tp', split_axis=0, concat_axis=1, tiled=True)]
    dot_general x4 -> x0, matrix products: 5.09 us -> none  [the longest x1 3.04 us: body(): jnp.dot(head_rows, lax.all_gather(w_out, 'tp', axis=0, tiled=True), prefe...]
    slice x5 -> x0, local copies, waits for them, and re-layouts: 3.21 us -> none  [the longest x2 1.38 us: body(): key_blocks[:-1]]
    ppermute x1 -> x0, starting transfers between devices: 3.12 us -> none  [shifted(): return lax.ppermute(block, axis, route)]
  transfers between devices with their start and end apart: 3 -> 0, of which waited for: 2 -> 0; matrix products, arithmetic and copies ran while one was open for 5% -> 0% of each run, Pallas kernels for 0% -> 0%
where the time goes in v2:
time: 186 us; the launch traced here: 185 us
  Pallas kernels  181 us (97%)
  other arithmetic  2.06 us (1%)
  local copies, waits for them, and re-layouts  1.88 us (1%)
    pallas_call x1, Pallas kernels, layer(): pl.pallas_call(layer_kernel, name='layer', out_shape=jax.ShapeDtypeStruct...  181 us

profile of v2, /device:TPU:27, one launch (start us, length us, event | category | flops | bytes accessed | tf_op | source)
XLA Modules:
  0.0 185.4 jit_solution(12636410558692165660)
XLA Ops:
  0.0 0.7 convert_bitcast_fusion
  0.7 1.3 pad_maximum_fusion.info
  2.1 181.4 %layer.1 = bf16[128,2048]{1,0:T(8,128)(2,1)} custom-call(bf16[1024,128]{1,0:T(8,128)(2,1)} %queries.1, f32[2]{0:T(128)} %sinks.1, f32[8,1024]{1,0:T(8,128)} %pad_maximum_fusion.info, f32[1,2048]{1,0:T(1,128)} %bitcast.5, bf16[1024,256]{1,0:T(8,128)(2,1)} %keys.1, bf16[1024,256]{1,0:T(8,128)(2,1)} %values.1, bf16[128,2048]{1,0:T(8,128)(2,1)} %w_out.1, ...), custom_call_target="tpu_custom_call" | custom-call | flops 19327352832 | bytes 9437184 | tf_op jit(solution)/shard_map/layer/pallas_call | solution.py:658
  183.5 1.9 %copy.17 = bf16[128,2048]{1,0:T(8,128)(2,1)} copy(bf16[128,2048]{1,0:T(8,128)(2,1)} %layer.1) | data formatting | bytes 1048576

commit v3 on v2

v3 whole, which is shorter than its diff:
```python
import functools

import jax
import jax.numpy as jnp
from jax import lax
from jax.experimental import pallas as pl
from jax.experimental.pallas import tpu as pltpu
from jax.sharding import PartitionSpec as P

HD = 64
GROUP = 4
WINDOW = 128
TOPK = 4
CHUNKS = 8
TILE = 256
MESH = pl.DeviceIdType.MESH
F32 = jnp.float32
BF16 = jnp.bfloat16
NT = (((1,), (1,)), ((), ()))


def dot(a, b):
    return jnp.dot(a, b, preferred_element_type=F32)


def dot_t(a, b):
    return lax.dot_general(a, b, NT, preferred_element_type=F32)


def silu(v):
    return v / (1.0 + jnp.exp(jnp.minimum(-v, 87.0)))


def loop(n, body):
    lax.fori_loop(0, n, lambda i, carry: (body(i), carry)[1], 0)


def layer_kernel(
    queries,
    sinks,
    ids,
    route_weights,
    gain,
    keys,
    values,
    w_out,
    residual,
    w_gate,
    w_up,
    w_down,
    s_gate,
    s_up,
    s_down,
    out,
    wg,
    wu,
    wd,
    sgu,
    sd,
    gathered,
    onehot,
    mix,
    sent,
    arrived,
    hidden,
    acc_g,
    acc_u,
    sh_acc,
    sh,
    returned,
    x_recv,
    z_recv,
    sends,
    locals_,
    w_recv,
    ag_recv,
    fw_recv,
    d_recv,
    r_recv,
    x_recv_sem,
    z_recv_sem,
    rim_send,
    rim_recv,
    wz_recv,
    wx_send,
    wx_recv,
    p_recv,
    k_ext,
    v_ext,
    attended,
    heads,
    after_mix,
    place_t,
    place,
):
    n_sp = lax.axis_size("sp")
    n_tp = lax.axis_size("tp")
    lanes = n_tp // 2
    s = lax.axis_index("sp")
    t = lax.axis_index("tp")
    z = t // 2
    core = t % 2
    rows = after_mix.shape[0]
    width = after_mix.shape[1]
    head_cols = w_out.shape[0]
    seq_rows = n_tp * rows
    chunks, _, _, step = gathered.shape
    half_cap = sent.shape[2]
    slots = n_sp * half_cap
    ff = wg.shape[1] // 2
    sff = sd.shape[1]
    bands = 2 * ff // TILE
    per = step // TILE

    def sp_index(j):
        other, bit = s, 1
        while bit < n_sp:
            if j // bit % 2:
                other = other + bit - 2 * bit * (s // bit % 2)
            bit *= 2
        return other

    def sp_peer(j):
        return {"sp": sp_index(j)}

    def z_peer(j):
        return {"tp": ((z + j) % lanes) * 2 + core}

    partner = {"tp": z * 2 + 1 - core}

    barrier = pltpu.get_barrier_semaphore()
    for j in range(1, n_sp):
        pl.semaphore_signal(barrier, inc=1, device_id=sp_peer(j), device_id_type=MESH)
    for j in range(1, lanes):
        pl.semaphore_signal(barrier, inc=1, device_id=z_peer(j), device_id_type=MESH)
    pl.semaphore_signal(barrier, inc=1, device_id=partner, device_id_type=MESH)

    def cols(c):
        return pl.ds(pl.multiple_of(c * step, step), step)

    def remote(src, dst, send, recv, peer):
        return pltpu.make_async_remote_copy(
            src_ref=src, dst_ref=dst, send_sem=send, recv_sem=recv, device_id=peer, device_id_type=MESH
        )

    def wait_bytes(ref, sem):
        remote(ref, ref, sem, sem, partner).wait_recv()

    def is_far(j):
        gap = (z + j) % lanes - z
        return (gap * gap == (lanes - 1) ** 2) & (lanes > 2)

    def from_nearest(k):
        low = jnp.where(k >= z, k + 1, k)
        high = lanes - 1 - jnp.where(k >= lanes - 1 - z, k + 1, k)
        return jnp.where(2 * z < lanes, low, high)

    edge = (z % (lanes - 1) == 0) & (lanes > 2)
    relay_up = (z == lanes - 2) & (lanes > 2)
    relay_down = (z == 1) & (lanes > 2)

    def own_piece(c, j):
        return remote(gathered.at[c, t], gathered.at[c, t], sends.at[0], ag_recv.at[c, z], z_peer(j))

    def first_far(j):
        block = gathered.at[0, t]
        return remote(block, block, sends.at[13], ag_recv.at[0, z], z_peer(j))

    def own_to_partner(c):
        return remote(gathered.at[c, t], gathered.at[c, t], sends.at[1], fw_recv.at[c], partner)

    def forward(c, source):
        block = gathered.at[c, source * 2 + core]
        return remote(block, block, sends.at[1], fw_recv.at[c], partner)

    def relay_piece(c, source, to, n):
        block = gathered.at[c, source * 2 + core]
        return remote(block, block, sends.at[n], ag_recv.at[c, source], {"tp": to * 2 + core})

    def dispatch(c, j):
        sem = d_recv.at[c + c // (chunks - 1) * j]
        return remote(sent.at[c, j], arrived.at[c, j], sends.at[2], sem, sp_peer(j))

    def give_back(c, j):
        return remote(sent.at[c, j], returned.at[c, j], sends.at[3], r_recv.at[c], sp_peer(j))

    def cross(c):
        return remote(gathered.at[c, 0:lanes], x_recv.at[c], sends.at[4], x_recv_sem.at[c], partner)

    def spread(c, j):
        block = gathered.at[c, lanes + (z + j) % lanes]
        return remote(block, z_recv.at[c, j], sends.at[5], z_recv_sem.at[c], z_peer(j))

    weights = ((w_gate, wg), (w_up, wu), (w_down, wd))
    shared = (
        (s_gate, lambda c: sgu.at[c, 0:sff]),
        (s_up, lambda c: sgu.at[c, sff : 2 * sff]),
        (s_down, lambda c: sd.at[c]),
    )

    def own_weight(n, c):
        src, dst = weights[n]
        return pltpu.make_async_copy(src.at[0, :, cols(c)], dst.at[c, 0:ff], locals_.at[n // 2])

    def other_weight(n, c):
        src, dst = weights[n]
        block = dst.at[c, ff : 2 * ff]
        return remote(src.at[0, :, cols(c)], block, sends.at[6 + n // 2], w_recv.at[n // 2], partner)

    def shared_weight(n, c):
        src, dst = shared[n]
        return pltpu.make_async_copy(src.at[:, cols(c)], dst(c), locals_.at[2 + n // 2])

    group_width = min(width // n_sp, step)
    groups = width // group_width // n_sp

    def group_at(sp, g, lane):
        first = (sp * groups + g) * group_width
        band = pl.ds(pl.multiple_of(first % step, group_width), group_width)
        return wd.at[first // step, pl.ds(pl.multiple_of(lane * head_cols, head_cols), head_cols), band]

    def out_shard(g, j):
        block = group_at(s, g, z)
        return remote(block, block, sends.at[8], wz_recv.at[g, z], z_peer(j))

    def out_along(g, source, to, n):
        block = group_at(s, g, source)
        return remote(block, block, sends.at[n], wz_recv.at[g, source], {"tp": to * 2 + core})

    def out_relay(g, source, i):
        block = group_at(s, g, source)
        return remote(block, block, wx_send.at[i], wx_recv.at[i], sp_peer(i))

    some_pieces = wd.at[0:groups, 0 : (lanes - 1) * head_cols, 0:group_width]
    fewer_pieces = wd.at[0:groups, 0 : (lanes - 2) * head_cols, 0:group_width]
    relay_pieces = wd.at[0:groups, 0:head_cols, 0:group_width]

    def out_own(c):
        mine = wd.at[c, pl.ds(pl.multiple_of(z * head_cols, head_cols), head_cols)]
        return pltpu.make_async_copy(w_out.at[:, cols(c)], mine, locals_.at[4])

    kv_start = t * head_cols // HD // GROUP * HD
    kv_cols = pl.ds(pl.multiple_of(kv_start // 128 * 128, 128), 128)
    parity = kv_start // HD % 2

    def rim(src, dst, n):
        last = src.at[pl.ds(seq_rows - WINDOW, WINDOW), kv_cols]
        return remote(last, dst.at[0:WINDOW], rim_send.at[n], rim_recv.at[n], {"sp": (s + 1) % n_sp})

    def own_kv(src, dst, n):
        return pltpu.make_async_copy(src.at[:, kv_cols], dst.at[WINDOW : WINDOW + seq_rows], locals_.at[5 + n])

    own_residual = pltpu.make_async_copy(residual, after_mix, locals_.at[7])
    own_kv(keys, k_ext, 0).start()
    own_kv(values, v_ext, 1).start()
    own_residual.start()

    loop(chunks, lambda c: out_own(c).start())

    def start_local(c):
        for n in range(2):
            own_weight(n, c).start()
        for n in range(3):
            shared_weight(n, c).start()

    loop(chunks, start_local)

    pltpu.make_async_copy(wd.at[:, 0:head_cols], wd.at[:, 0:head_cols], locals_.at[4]).wait()
    pl.semaphore_wait(barrier, n_sp - 1 + lanes - 1 + 1)
    for g in range(groups):
        for j in range(1, lanes):

            @pl.when(jnp.logical_not(is_far(j)))
            def _():
                out_shard(g, j).start()

    rim(keys, k_ext, 0).start()
    rim(values, v_ext, 1).start()

    def start_other(c):
        for n in range(3):
            other_weight(n, c).start()

    loop(chunks, start_other)
    own_kv(keys, k_ext, 0).wait()
    own_kv(values, v_ext, 1).wait()

    lane_id = lax.broadcasted_iota(jnp.int32, (1, 128), 1)
    query_row = lax.broadcasted_iota(jnp.int32, (2 * rows, 1), 0)
    in_block = query_row % rows
    key_at = lax.broadcasted_iota(jnp.int32, (1, rows + WINDOW), 1)
    band_mask = (key_at <= in_block + WINDOW) & (key_at > in_block)
    sink = jnp.where(query_row < rows, sinks[0], sinks[1])

    def attend(block):
        first = pl.multiple_of(block * rows, rows)

        @pl.when(block == 0)
        def _():
            rim(keys, k_ext, 0).wait_recv()
            rim(values, v_ext, 1).wait_recv()

        q = queries[pl.ds(first, rows), :].astype(F32) * HD ** (-0.5)
        turned = pltpu.roll(q, 64, 1)
        mine = lane_id // HD == parity
        q0 = jnp.where(mine, jnp.where(parity == 0, q, turned), 0.0)
        q1 = jnp.where(mine, jnp.where(parity == 1, q, turned), 0.0)
        q2 = jnp.concatenate([q0, q1], axis=0).astype(BF16)
        scores = dot_t(q2, k_ext[pl.ds(first, rows + WINDOW), :])
        allowed = band_mask & (s * seq_rows + first + key_at >= WINDOW)
        scores = jnp.where(allowed, scores, -1e30)
        top = jnp.maximum(jnp.max(scores, axis=1, keepdims=True), sink)
        exps = jnp.exp(scores - top)
        total = jnp.sum(exps, axis=1, keepdims=True) + jnp.exp(sink - top)
        probs = (exps / total).astype(BF16)
        o = dot(probs, v_ext[pl.ds(first, rows + WINDOW), :])
        o0, o1 = o[0:rows], o[rows : 2 * rows]
        o0 = jnp.where(parity == 0, o0, pltpu.roll(o0, 64, 1))
        o1 = jnp.where(parity == 1, o1, pltpu.roll(o1, 64, 1))
        return jnp.where(lane_id < HD, o0, o1).astype(BF16)

    def head_rows(j):
        return remote(attended.at[j], heads.at[z], sends.at[9], rim_recv.at[2], z_peer(j))

    def attend_chip(i):
        j = (i + 1) % lanes
        other = (z + j) % lanes

        def half(n):
            value = attend(other * 2 + n)

            @pl.when(j > 0)
            def _():
                attended[j, pl.ds(pl.multiple_of(n * rows, rows), rows), :] = value

            @pl.when(j == 0)
            def _():
                heads[z, pl.ds(pl.multiple_of(n * rows, rows), rows), :] = value

        loop(2, half)

    loop(lanes, attend_chip)

    def relay_shards(k):
        source = from_nearest(k)
        for g in range(groups):
            wait_bytes(group_at(s, g, source), wz_recv.at[g, source])

            @pl.when(relay_up & (source == 0))
            def _():
                out_along(g, 0, lanes - 1, 10).start()

            @pl.when(relay_down & (source == lanes - 1))
            def _():
                out_along(g, lanes - 1, 0, 11).start()

            for i in range(n_sp - 1, 0, -1):
                out_relay(g, source, i).start()

    loop(lanes - 2, relay_shards)
    for j in range(1, lanes):
        head_rows(j).start()
    relay_shards(lanes - 2)

    lane_q = lax.broadcasted_iota(jnp.int32, (1, seq_rows), 1)
    named_rows, weight_rows = [], []
    for j in range(n_sp):
        hit = ids[...] == sp_index(j) * lanes + z
        named_rows.append(jnp.max(jnp.where(hit, 1.0, 0.0), axis=0, keepdims=True))
        weight_rows.append(jnp.sum(jnp.where(hit, route_weights[...], 0.0), axis=0, keepdims=True))
    fill = [jnp.zeros((1, seq_rows), F32)] * (-n_sp % 8)
    named = jnp.concatenate(named_rows + fill, axis=0)
    scan = named
    apart = 1
    while apart < seq_rows:
        scan = scan + jnp.where(lane_q >= apart, pltpu.roll(scan, apart, 1), 0.0)
        apart *= 2
    half_at = (core * half_cap).astype(F32)
    places = jnp.where(named > 0, scan - named - half_at, -1.0)
    for j in range(n_sp):
        place_t[j] = places[j : j + 1]
    place[...] = jnp.concatenate([places] + weight_rows + fill, axis=0).T.reshape(place.shape)

    slot_down = lax.broadcasted_iota(jnp.int32, (half_cap, 1), 0).astype(F32)
    slot_along = lax.broadcasted_iota(jnp.int32, (1, half_cap), 1).astype(F32)

    def build_pick(j):
        hit = place_t[j] == slot_down
        onehot[j] = jnp.where(hit, 1.0, 0.0).astype(BF16)

    loop(n_sp, build_pick)

    spot = places.shape[0]

    def build_mix(i):
        for j in range(n_sp):
            hit = place[i, :, j : j + 1] == slot_along
            part = jnp.where(hit, place[i, :, spot + j : spot + j + 1], 0.0).astype(BF16)
            at = pl.ds(pl.multiple_of(i // 2 * rows, rows), rows)
            mix[i % 2, at, j * half_cap : (j + 1) * half_cap] = part

    loop(n_tp, build_mix)


    wait_bytes(heads.at[1:lanes], rim_recv.at[2])
    own_residual.wait()

    def wait_relays(i):
        if i == 0:
            return
        wait_bytes(some_pieces, wx_recv.at[i])

    def stripe(c):
        return pl.ds(pl.multiple_of(c * per * rows, per * rows), per * rows)

    def exchange(c):
        return remote(
            acc_g.at[1 - core, stripe(c)], acc_g.at[2, stripe(c)], sends.at[12], p_recv.at[c], partner
        )

    def project(c):
        parts = [
            dot(heads[i][:, 0:head_cols], wd[c, i * head_cols : (i + 1) * head_cols, :]) for i in range(lanes)
        ]
        value = sum(parts[1:], parts[0])
        for n in range(2):
            for p in range(per):
                at = pl.ds(pl.multiple_of((c * per + p) * rows, rows), rows)
                acc_g[n, at, :] = value[n * rows : (n + 1) * rows, p * TILE : (p + 1) * TILE]
        exchange(c).start()

    if chunks % n_sp == 0:
        for i in range(n_sp):
            wait_relays(i)
            for n in range(chunks // n_sp):
                project(sp_index(i) * (chunks // n_sp) + n)
    else:
        for i in range(n_sp):
            wait_relays(i)
        loop(chunks, project)
    for i in range(1, n_sp):
        wait_bytes(some_pieces, wx_send.at[i])

    @pl.when(edge)
    def _():
        wait_bytes(fewer_pieces, sends.at[8])

    @pl.when(jnp.logical_not(edge))
    def _():
        wait_bytes(some_pieces, sends.at[8])

    @pl.when(relay_up)
    def _():
        wait_bytes(relay_pieces, sends.at[10])

    @pl.when(relay_down)
    def _():
        wait_bytes(relay_pieces, sends.at[11])

    for c in range(chunks):
        own_weight(2, c).start()
    def start_pieces(c):
        own_to_partner(c).start()
        for j in range(1, lanes):

            @pl.when(jnp.logical_not(is_far(j)))
            def _():
                own_piece(c, j).start()

            if isinstance(c, int) and c == 0:

                @pl.when(is_far(j))
                def _():
                    first_far(j).start()


    squares = jnp.zeros((rows, 1), F32)
    for c in range(chunks):
        exchange(c).wait_recv()
        for p in range(per):
            k = c * per + p
            at = pl.ds(k * rows, rows)
            band = slice(k * TILE, (k + 1) * TILE)
            value = after_mix[:, band].astype(F32) + (acc_g[core, at, :] + acc_g[2, at, :])
            value = value.astype(BF16)
            after_mix[:, band] = value
            squares += jnp.sum(value.astype(F32) * value.astype(F32), axis=1, keepdims=True)
    scale = lax.rsqrt(squares / width + 1e-06)
    for c in range(chunks):
        band = slice(c * step, (c + 1) * step)
        gathered[c, t] = (after_mix[:, band].astype(F32) * scale * gain[:, band]).astype(BF16)
        if c < 2:
            start_pieces(c)
    wait_bytes(acc_g.at[2, 0 : chunks * per * rows], sends.at[12])

    def gather_chunk(c):
        for k in range(lanes - 1):
            source = from_nearest(k)
            wait_bytes(gathered.at[c, source], ag_recv.at[c, source])

            @pl.when(relay_up & (source == 0) & (c > 0))
            def _():
                relay_piece(c, 0, lanes - 1, 10).start()

            @pl.when(relay_down & (source == lanes - 1) & (c > 0))
            def _():
                relay_piece(c, lanes - 1, 0, 11).start()

            forward(c, source).start()
        wait_bytes(gathered.at[c, 0:lanes], fw_recv.at[c])

    def pick_chunk(c):
        block = gathered[c].reshape(n_tp * rows, step)
        picked = dot(onehot[...].reshape(slots, seq_rows), block).astype(BF16)
        picked = picked.reshape(n_sp, half_cap, step)
        sent[c] = picked
        for j in range(n_sp - 1, 0, -1):
            dispatch(c, j).start()
        arrived[c, 0] = picked[0]

    def shared_chunk(c, first):
        block = gathered[c].reshape(n_tp * rows, step)
        value = dot_t(block, sgu[c])
        sh_acc[...] = value if first else sh_acc[...] + value

    def expert_chunk(c, first):
        wait_bytes(arrived.at[c, 1:n_sp], d_recv.at[c])
        lhs = arrived[c].reshape(slots, step)

        def one(i):
            band = pl.ds(pl.multiple_of(i * TILE, TILE), TILE)
            for w, acc in ((wg, acc_g), (wu, acc_u)):
                value = dot_t(lhs, w[c, band, :])
                acc[i] = value if first else acc[i] + value

        loop(bands, one)

    def last_rows(c, j):
        lhs = arrived[c, j]
        mine = slice(j * half_cap, (j + 1) * half_cap)
        for i in range(bands):
            band = slice(i * TILE, (i + 1) * TILE)
            g = acc_g[i, mine] + dot_t(lhs, wg[c, band, :])
            u = acc_u[i, mine] + dot_t(lhs, wu[c, band, :])
            hidden[j, :, band] = (silu(g) * u).astype(BF16)

    def dispatch_step(c, depth):
        gather_chunk(c)
        if isinstance(c, int):
            if c + 2 < chunks:
                start_pieces(c + 2)
        else:

            @pl.when(c + 2 < chunks)
            def _():
                start_pieces(c + 2)

        pick_chunk(c)
        shared_chunk(c, depth == 0)
        if depth > 1:
            expert_chunk(c - 2, depth == 2)

    def wait_local(ref, n):
        pltpu.make_async_copy(ref, ref, locals_.at[n]).wait()

    wait_local(sgu, 2)
    dispatch_step(0, 0)
    dispatch_step(1, 1)
    wait_local(wg, 0)
    wait_bytes(wg, w_recv.at[0])
    dispatch_step(2, 2)
    lax.fori_loop(3, chunks, lambda c, carry: (dispatch_step(c, 3), carry)[1], 0)
    expert_chunk(chunks - 2, False)
    shared_value = silu(sh_acc[:, 0:sff]) * sh_acc[:, sff : 2 * sff]
    shared_value = shared_value.astype(BF16)
    for i in range(n_tp):
        sh[i % 2, i // 2 * rows : (i // 2 + 1) * rows] = shared_value[i * rows : (i + 1) * rows]
    last_rows(chunks - 1, 0)

    wait_local(wd.at[:, 0:ff], 1)
    wait_bytes(wd.at[:, ff : 2 * ff], w_recv.at[1])
    for j in range(1, n_sp):
        dispatch(chunks - 1, j).wait_recv()
        last_rows(chunks - 1, j)
        if j == 1:
            wait_bytes(sent.at[:, 1:n_sp], sends.at[2])
        sent[0, j] = dot(hidden[j], wd[0]).astype(BF16)
        give_back(0, j).start()
    returned[0, 0] = dot(hidden[0], wd[0]).astype(BF16)

    def down_chunk(c):
        value = dot(hidden[...].reshape(slots, 2 * ff), wd[c]).astype(BF16)
        value = value.reshape(n_sp, half_cap, step)
        sent[c] = value
        for j in range(n_sp - 1, 0, -1):
            give_back(c, j).start()
        returned[c, 0] = value[0]

    down_chunk(1)
    wait_bytes(gathered.at[:, 0:lanes], sends.at[1])

    @pl.when(edge)
    def _():
        wait_bytes(gathered.at[:, 0 : lanes - 2], sends.at[0])
        wait_bytes(gathered.at[0, 0], sends.at[13])

    @pl.when(jnp.logical_not(edge))
    def _():
        wait_bytes(gathered.at[:, 0 : lanes - 1], sends.at[0])

    @pl.when(relay_up)
    def _():
        wait_bytes(gathered.at[1:chunks, 0], sends.at[10])

    @pl.when(relay_down)
    def _():
        wait_bytes(gathered.at[1:chunks, 0], sends.at[11])

    wait_local(sd, 3)

    def combine_chunk(c):
        wait_bytes(returned.at[c, 1:n_sp], r_recv.at[c])
        held = returned[c].reshape(slots, step)

        def part(p):
            return (dot(mix[p], held) + dot(sh[p], sd[c])).reshape(lanes, rows, step)

        gathered[c, 0:lanes] = part(1 - core).astype(BF16)
        cross(c).start()

        if c + 2 < chunks:
            down_chunk(c + 2)

        here = part(core)
        cross(c).wait_recv()
        gathered[c, lanes : 2 * lanes] = (here + x_recv[c].astype(F32)).astype(BF16)
        for j in range(1, lanes):
            spread(c, j).start()

    for c in range(chunks):
        combine_chunk(c)

    def finish_chunk(c):
        total = gathered[c, lanes + z].astype(F32)
        wait_bytes(z_recv.at[c, 1:lanes], z_recv_sem.at[c])
        for j in range(1, lanes):
            total += z_recv[c, j].astype(F32)
        out[:, cols(c)] = (after_mix[:, cols(c)].astype(F32) + total).astype(BF16)

    loop(chunks, finish_chunk)

    wait_bytes(gathered.at[:, 0 : lanes - 1], sends.at[5])
    wait_bytes(sent.at[:, 1:n_sp], sends.at[3])
    wait_bytes(gathered.at[:, 0:lanes], sends.at[4])
    wait_bytes(wg, sends.at[6])
    wait_bytes(wd.at[:, ff : 2 * ff], sends.at[7])
    wait_bytes(attended.at[1:lanes], sends.at[9])
    rim(keys, k_ext, 0).wait_send()
    rim(values, v_ext, 1).wait_send()


def layer(
    queries, sinks, ids, route_weights, gain, keys, values, w_out, residual, w_gate, w_up, w_down, s_gate, s_up, s_down
):
    n_sp = lax.axis_size("sp")
    n_tp = lax.axis_size("tp")
    lanes = n_tp // 2
    rows, width = residual.shape
    step = width // CHUNKS
    ff = w_gate.shape[1]
    sff = s_gate.shape[0]
    q = rows * n_tp
    half_cap = max(2, 2 * q * TOPK // (n_sp * lanes)) // 2
    slots = n_sp * half_cap
    groups = width // min(width // n_sp, step) // n_sp
    padded = -(-n_sp // 8) * 8
    dma = pltpu.SemaphoreType.DMA
    vm = pltpu.VMEM
    in_vmem = pl.BlockSpec(memory_space=pltpu.VMEM)
    in_smem = pl.BlockSpec(memory_space=pltpu.SMEM)
    in_hbm = pl.BlockSpec(memory_space=pl.ANY)
    scratch = [
        vm((CHUNKS, 2 * ff, step), BF16),
        vm((CHUNKS, 2 * ff, step), BF16),
        vm((CHUNKS, 2 * ff, step), BF16),
        vm((CHUNKS, 2 * sff, step), BF16),
        vm((CHUNKS, sff, step), BF16),
        vm((CHUNKS, n_tp, rows, step), BF16),
        vm((n_sp, half_cap, q), BF16),
        vm((2, lanes * rows, slots), BF16),
        vm((CHUNKS, n_sp, half_cap, step), BF16),
        vm((CHUNKS, n_sp, half_cap, step), BF16),
        vm((n_sp, half_cap, 2 * ff), BF16),
        vm((2 * ff // TILE, slots, TILE), F32),
        vm((2 * ff // TILE, slots, TILE), F32),
        vm((q, 2 * sff), F32),
        vm((2, lanes * rows, sff), BF16),
        vm((CHUNKS, n_sp, half_cap, step), BF16),
        vm((CHUNKS, lanes, rows, step), BF16),
        vm((CHUNKS, lanes, rows, step), BF16),
        dma((14,)),
        dma((8,)),
        dma((2,)),
        dma((CHUNKS, lanes)),
        dma((CHUNKS,)),
        dma((CHUNKS + n_sp,)),
        dma((CHUNKS,)),
        dma((CHUNKS,)),
        dma((CHUNKS,)),
        dma((2,)),
        dma((3,)),
        dma((groups, lanes)),
        dma((n_sp,)),
        dma((n_sp,)),
        dma((CHUNKS,)),
        vm((q + WINDOW, 128), BF16),
        vm((q + WINDOW, 128), BF16),
        vm((lanes, 2 * rows, 128), BF16),
        vm((lanes, 2 * rows, 128), BF16),
        vm((rows, width), BF16),
        vm((n_sp, 1, q), F32),
        vm((n_tp, rows, 2 * padded), F32),
    ]
    return pl.pallas_call(
        layer_kernel,
        name="layer",
        out_shape=jax.ShapeDtypeStruct((rows, width), BF16),
        in_specs=[in_vmem, in_smem, in_vmem, in_vmem, in_vmem] + [in_hbm] * 10,
        out_specs=in_vmem,
        scratch_shapes=scratch,
        compiler_params=pltpu.CompilerParams(
            collective_id=0, has_side_effects=True, vmem_limit_bytes=67043328
        ),
        cost_estimate=pl.CostEstimate(
            flops=12 * slots * ff * width, bytes_accessed=6 * ff * width, transcendentals=0
        ),
    )(queries, sinks, ids, route_weights, gain, keys, values, w_out, residual, w_gate, w_up, w_down, s_gate, s_up, s_down)


def body(
    queries,
    keys,
    values,
    sink_logits,
    w_out,
    residual,
    norm_gain,
    expert_ids,
    expert_weights,
    w_gate,
    w_up,
    w_down,
    shared_gate,
    shared_up,
    shared_down,
):
    spare = 128 - queries.shape[1]
    if spare > 0:
        queries = jnp.pad(queries, ((0, 0), (0, spare)))
        sink_logits = jnp.pad(sink_logits, (0, spare // HD))
    return layer(
        queries,
        sink_logits,
        expert_ids.T,
        expert_weights.T,
        norm_gain[None],
        keys,
        values,
        w_out,
        residual,
        w_gate,
        w_up,
        w_down,
        shared_gate,
        shared_up,
        shared_down,
    )


def solution(mesh):
    return jax.shard_map(
        body,
        mesh=mesh,
        in_specs=(
            P("sp", "tp"),
            P("sp", None),
            P("sp", None),
            P("tp"),
            P("tp", None),
            P(("sp", "tp"), None),
            P(),
            P("sp", None),
            P("sp", None),
            P(("sp", "tp"), None, None),
            P(("sp", "tp"), None, None),
            P(("sp", "tp"), None, None),
            P("tp", None),
            P("tp", None),
            P("tp", None),
        ),
        out_specs=P(("sp", "tp"), None),
        check_vma=False,
    )
```

time: 186 us -> 158 us (0.85)
  Pallas kernels: 181 us -> 155 us
  other arithmetic: 2.06 us -> 0 us
    pallas_call x1, Pallas kernels: 181 us -> 155 us  [layer(): pl.pallas_call(layer_kernel, name='layer', out_shape=jax.ShapeDtypeStruct...]
where the time goes in v3:
time: 158 us; the launch traced here: 157 us
  Pallas kernels  155 us (98%)
  local copies, waits for them, and re-layouts  1.88 us (1%)
    pallas_call x1, Pallas kernels, layer(): pl.pallas_call(layer_kernel, name='layer', out_shape=jax.ShapeDtypeStruct...  155 us

profile of v3, /device:TPU:27, one launch (start us, length us, event | category | flops | bytes accessed | tf_op | source)
XLA Modules:
  0.0 156.7 jit_solution(13494179284740785767)
XLA Ops:
  0.0 154.8 %layer.1 = bf16[128,2048]{1,0:T(8,128)(2,1)} custom-call(bf16[1024,128]{1,0:T(8,128)(2,1)} %queries.1, f32[2]{0:T(128)} %sinks.1, s32[4,1024]{1,0:T(4,128)} %bitcast.3, f32[4,1024]{1,0:T(4,128)} %bitcast.4, f32[1,2048]{1,0:T(1,128)} %bitcast.5, bf16[1024,256]{1,0:T(8,128)(2,1)} %keys.1, bf16[1024,256]{1,0:T(8,128)(2,1)} %values.1, bf16[128,2048]{1,0:T(8,128)(2,1)} %w_out.1, ...), custom_call_target="tpu_custom_call" | custom-call | flops 19327352832 | bytes 9437184 | tf_op jit(solution)/shard_map/layer/pallas_call | solution.py:724
  154.8 1.9 %copy.17 = bf16[128,2048]{1,0:T(8,128)(2,1)} copy(bf16[128,2048]{1,0:T(8,128)(2,1)} %layer.1) | data formatting | bytes 1048576

commit v4 on v3

--- a/solution.py
+++ b/solution.py
@@ -36,11 +36,11 @@
 
 
 def layer_kernel(
-    queries,
-    sinks,
-    ids,
-    route_weights,
-    gain,
+    queries_in,
+    sinks_in,
+    ids_in,
+    route_in,
+    gain_in,
     keys,
     values,
     w_out,
@@ -85,6 +85,11 @@
     wx_send,
     wx_recv,
     p_recv,
+    queries,
+    sinks,
+    ids,
+    route_weights,
+    gain,
     k_ext,
     v_ext,
     attended,
@@ -251,11 +256,25 @@
         return pltpu.make_async_copy(src.at[:, kv_cols], dst.at[WINDOW : WINDOW + seq_rows], locals_.at[5 + n])
 
     own_residual = pltpu.make_async_copy(residual, after_mix, locals_.at[7])
+    loop(chunks, lambda c: out_own(c).start())
+    small = [
+        pltpu.make_async_copy(src, dst, locals_.at[8 + n])
+        for n, (src, dst) in enumerate(
+            (
+                (queries_in, queries),
+                (sinks_in, sinks),
+                (ids_in, ids),
+                (route_in, route_weights),
+                (gain_in, gain),
+            )
+        )
+    ]
+    for copy in small:
+        copy.start()
     own_kv(keys, k_ext, 0).start()
     own_kv(values, v_ext, 1).start()
     own_residual.start()
 
-    loop(chunks, lambda c: out_own(c).start())
 
     def start_local(c):
         for n in range(2):
@@ -282,6 +301,8 @@
             other_weight(n, c).start()
 
     loop(chunks, start_other)
+    for copy in small:
+        copy.wait()
     own_kv(keys, k_ext, 0).wait()
     own_kv(values, v_ext, 1).wait()
 
@@ -290,7 +311,7 @@
     in_block = query_row % rows
     key_at = lax.broadcasted_iota(jnp.int32, (1, rows + WINDOW), 1)
     band_mask = (key_at <= in_block + WINDOW) & (key_at > in_block)
-    sink = jnp.where(query_row < rows, sinks[0], sinks[1])
+    sink = jnp.where(query_row < rows, sinks[:, 0:1], sinks[:, 1:2])
 
     def attend(block):
         first = pl.multiple_of(block * rows, rows)
@@ -319,8 +340,10 @@
         o1 = jnp.where(parity == 1, o1, pltpu.roll(o1, 64, 1))
         return jnp.where(lane_id < HD, o0, o1).astype(BF16)
 
+    head_band = pl.ds(pl.multiple_of(z * 128, 128), 128)
+
     def head_rows(j):
-        return remote(attended.at[j], heads.at[z], sends.at[9], rim_recv.at[2], z_peer(j))
+        return remote(attended.at[j], heads.at[:, head_band], sends.at[9], rim_recv.at[2], z_peer(j))
 
     def attend_chip(i):
         j = (i + 1) % lanes
@@ -335,11 +358,11 @@
 
             @pl.when(j == 0)
             def _():
-                heads[z, pl.ds(pl.multiple_of(n * rows, rows), rows), :] = value
+                heads[pl.ds(pl.multiple_of(n * rows, rows), rows), head_band] = value
 
         loop(2, half)
 
-    loop(lanes, attend_chip)
+    loop(lanes - 1, attend_chip)
 
     def relay_shards(k):
         source = from_nearest(k)
@@ -357,7 +380,9 @@
             for i in range(n_sp - 1, 0, -1):
                 out_relay(g, source, i).start()
 
-    loop(lanes - 2, relay_shards)
+    relay_shards(0)
+    loop(1, lambda i: attend_chip(i + lanes - 1))
+    loop(lanes - 3, lambda k: relay_shards(k + 1))
     for j in range(1, lanes):
         head_rows(j).start()
     relay_shards(lanes - 2)
@@ -402,7 +427,7 @@
     loop(n_tp, build_mix)
 
 
-    wait_bytes(heads.at[1:lanes], rim_recv.at[2])
+    wait_bytes(heads.at[:, 0 : (lanes - 1) * 128], rim_recv.at[2])
     own_residual.wait()
 
     def wait_relays(i):
@@ -419,10 +444,17 @@
         )
 
     def project(c):
-        parts = [
-            dot(heads[i][:, 0:head_cols], wd[c, i * head_cols : (i + 1) * head_cols, :]) for i in range(lanes)
-        ]
-        value = sum(parts[1:], parts[0])
+        if head_cols == 128:
+            value = dot(heads[...], wd[c, 0 : lanes * head_cols, :])
+        else:
+            parts = [
+                dot(
+                    heads[:, i * 128 : i * 128 + head_cols],
+                    wd[c, i * head_cols : (i + 1) * head_cols, :],
+                )
+                for i in range(lanes)
+            ]
+            value = sum(parts[1:], parts[0])
         for n in range(2):
             for p in range(per):
                 at = pl.ds(pl.multiple_of((c * per + p) * rows, rows), rows)
@@ -677,7 +709,6 @@
     dma = pltpu.SemaphoreType.DMA
     vm = pltpu.VMEM
     in_vmem = pl.BlockSpec(memory_space=pltpu.VMEM)
-    in_smem = pl.BlockSpec(memory_space=pltpu.SMEM)
     in_hbm = pl.BlockSpec(memory_space=pl.ANY)
     scratch = [
         vm((CHUNKS, 2 * ff, step), BF16),
@@ -699,7 +730,7 @@
         vm((CHUNKS, lanes, rows, step), BF16),
         vm((CHUNKS, lanes, rows, step), BF16),
         dma((14,)),
-        dma((8,)),
+        dma((13,)),
         dma((2,)),
         dma((CHUNKS, lanes)),
         dma((CHUNKS,)),
@@ -713,10 +744,15 @@
         dma((n_sp,)),
         dma((n_sp,)),
         dma((CHUNKS,)),
+        vm((q, 128), BF16),
+        vm((1, 2), F32),
+        vm((TOPK, q), jnp.int32),
+        vm((TOPK, q), F32),
+        vm((1, width), F32),
         vm((q + WINDOW, 128), BF16),
         vm((q + WINDOW, 128), BF16),
         vm((lanes, 2 * rows, 128), BF16),
-        vm((lanes, 2 * rows, 128), BF16),
+        vm((2 * rows, lanes * 128), BF16),
         vm((rows, width), BF16),
         vm((n_sp, 1, q), F32),
         vm((n_tp, rows, 2 * padded), F32),
@@ -725,7 +761,7 @@
         layer_kernel,
         name="layer",
         out_shape=jax.ShapeDtypeStruct((rows, width), BF16),
-        in_specs=[in_vmem, in_smem, in_vmem, in_vmem, in_vmem] + [in_hbm] * 10,
+        in_specs=[in_hbm] * 15,
         out_specs=in_vmem,
         scratch_shapes=scratch,
         compiler_params=pltpu.CompilerParams(
@@ -760,7 +796,7 @@
         sink_logits = jnp.pad(sink_logits, (0, spare // HD))
     return layer(
         queries,
-        sink_logits,
+        sink_logits[None],
         expert_ids.T,
         expert_weights.T,
         norm_gain[None],

time: 158 us -> 157 us (level)
  Pallas kernels: 155 us -> 152 us
    pallas_call x1, Pallas kernels: 155 us -> 152 us  [layer(): pl.pallas_call(layer_kernel, name='layer', out_shape=jax.ShapeDtypeStruct...]
where the time goes in v4:
time: 157 us; the launch traced here: 154 us
  Pallas kernels  152 us (97%)
  local copies, waits for them, and re-layouts  1.88 us (1%)
    pallas_call x1, Pallas kernels, layer(): pl.pallas_call(layer_kernel, name='layer', out_shape=jax.ShapeDtypeStruct...  152 us

profile of v4, /device:TPU:27, one launch (start us, length us, event | category | flops | bytes accessed | tf_op | source)
XLA Modules:
  0.0 154.4 jit_solution(17093049717520164910)
XLA Ops:
  0.0 152.5 %layer.1 = bf16[128,2048]{1,0:T(8,128)(2,1)} custom-call(bf16[1024,128]{1,0:T(8,128)(2,1)} %queries_in.1, f32[1,2]{1,0:T(1,128)} %bitcast.7, s32[4,1024]{1,0:T(4,128)} %bitcast.4, f32[4,1024]{1,0:T(4,128)} %bitcast.5, f32[1,2048]{1,0:T(1,128)} %bitcast.6, bf16[1024,256]{1,0:T(8,128)(2,1)} %keys.1, bf16[1024,256]{1,0:T(8,128)(2,1)} %values.1, ...), custom_call_target="tpu_custom_call" | custom-call | flops 19327352832 | bytes 9437184 | tf_op jit(solution)/shard_map/layer/pallas_call | solution.py:760
  152.5 1.9 %copy.17 = bf16[128,2048]{1,0:T(8,128)(2,1)} copy(bf16[128,2048]{1,0:T(8,128)(2,1)} %layer.1) | data formatting | bytes 1048576
